TPU v7x, 32 devices: a whole 2x2x4 slice. The times are simulated.
32 devices in a mesh: rep: 2 (over x), fs: 8 (over z, y), tp: 2 (over core).
Axes of the slice: x: 2, y: 2, z: 4, core: 2. Of those that a mesh axis runs over, the one named last changes fastest.
Arguments:
- incoming_features: bfloat16 [3072, 2048], P(('rep', 'fs'), 'tp'), may hold values from -6 to 6
- attend_prenormal_scale: bfloat16 [2048], replicated, may hold values from 0.099609375 to 1.8984375
- probe_matrix: bfloat16 [2048, 512], P('fs', 'tp'), may hold values from -0.125 to 0.125
- lookup_matrix: bfloat16 [2048, 512], P('fs', 'tp'), may hold values from -0.125 to 0.125
- content_matrix: bfloat16 [2048, 1024], P('fs', 'tp'), may hold values from -0.125 to 0.125
- forgetting_matrix: bfloat16 [2048, 512], P('fs', 'tp'), may hold values from -0.125 to 0.125
- result_switch_matrix: bfloat16 [2048, 1024], P('fs', 'tp'), may hold values from -0.125 to 0.125
- forgetting_shift: float32 [512], P('tp'), may hold values from -0.5 to 5.5
- spike_forget_logarithm: float32 [3072, 512], P(('rep', 'fs'), 'tp'), may hold values from -0.7 to 0
- attend_unit_scale: bfloat16 [1024], P('tp'), may hold values from 0.099609375 to 1.8984375
- attend_result_matrix: bfloat16 [1024, 2048], P('tp', 'fs'), may hold values from -0.1875 to 0.1875
- perceptron_scale: bfloat16 [2048], replicated, may hold values from 0.099609375 to 1.8984375
- content_expand_matrix: bfloat16 [2048, 4096], P('fs', 'tp'), may hold values from -0.125 to 0.125
- switch_expand_matrix: bfloat16 [2048, 4096], P('fs', 'tp'), may hold values from -0.125 to 0.125
- content_kernel: bfloat16 [3, 4096], P(None, 'tp'), may hold values from -3.5 to 3.5
- switch_kernel: bfloat16 [3, 4096], P(None, 'tp'), may hold values from -3.5 to 3.5
- contract_matrix: bfloat16 [4096, 2048], P('tp', 'fs'), may hold values from -0.09375 to 0.09375
Outputs:
- out_rows: bfloat16 [3072, 2048], P(('rep', 'fs'), 'tp')
All inputs are finite; a program needn't handle non-finite values.
Results may differ from a plain program's by a relative error of at most 0.02.
Values may be sent and summed in bfloat16 or wider, within the bound.
A program may use at most 64 MiB of HBM per device.

v0:
```python
import functools

import jax
import jax.numpy as jnp
from jax import lax
from jax.experimental import pallas as pl
from jax.experimental.pallas import tpu as pltpu
from jax.sharding import PartitionSpec as P

HEAD_K = 32
HEAD_V = 64
SUB = 16

norm_eps = 1e-06
switch_multiplier = 16.0
MESH = pl.DeviceIdType.MESH
F32 = jnp.float32
BF16 = jnp.bfloat16
HIGHEST = lax.Precision.HIGHEST
VMEM_LIMIT = 60 * 1024 * 1024


def row_norm(content_tokens, gain):
    content_tokens = content_tokens.astype(F32)
    scaled = content_tokens * lax.rsqrt(
        jnp.mean(content_tokens * content_tokens, axis=-1, keepdims=True) + norm_eps
    )
    return (scaled * gain.astype(F32)).astype(BF16)


def factor(n):
    inner = 1
    for size in range(1, n + 1):
        if n % size == 0 and size * size <= n:
            inner = size
    return n // inner, inner


def place(ref, axis, index, size):
    at = pl.ds(pl.multiple_of(index * size, size), size)
    return ref.at[at, :] if axis == 0 else ref.at[:, at]


def send_to(source, target, send_sem, recv_sem, peer):
    copy = pltpu.make_async_remote_copy(
        src_ref=source,
        dst_ref=target,
        send_sem=send_sem,
        recv_sem=recv_sem,
        device_id=peer,
        device_id_type=MESH,
    )
    copy.start()
    return copy


def pieces_of(rows, most):
    for count in range(most, 1, -1):
        if rows % (16 * count) == 0:
            return count
    return 1


def first_half(
    project, result, expand, contract, features, gain, shift, spike, scale, axis, inside, sizes
):
    n_rep, n_fs, n_tp = sizes
    outer, inner = factor(n_fs)
    length, columns = features.shape
    rows = length * n_rep
    heads = shift.shape[0] // HEAD_K
    value_lanes = heads * HEAD_V
    group = n_rep * n_tp
    most = max(n_rep, n_tp)
    weights = (project, result, expand, contract)
    axes = (0, axis, 0, axis)
    splits = (2, 1, 4, 4)
    full = []
    chunks = []
    for w in range(4):
        shape = list(weights[w].shape)
        size = shape[0]
        shape[axes[w]] *= n_fs
        full.append(tuple(shape))
        split = pieces_of(size, splits[w])
        chunks += [(w, k * (size // split), size // split) for k in range(split)]
    count = len(chunks)

    def kernel(*refs):
        sources = refs[:4]
        features_ref, gain_ref, shift_ref, spike_ref, scale_ref = refs[4:9]
        if inside:
            expand_out, contract_out, middle_ref, mid_ref = refs[9:13]
            rest = refs[13:]
            result_out, gated_ref, partial_ref, slot_a, held, slot_b = rest[:6]
            rest = rest[6:]
        else:
            expand_out, contract_out, result_out, gated_ref = refs[9:13]
            rest = refs[13:]
        project_out, whole_ref = rest[:2]
        far_send, far_recv, near_send, near_recv, own_sem, group_send, group_recv = rest[2:9]
        if inside:
            sum_send, sum_recv = rest[9:]
        outs = (project_out, result_out, expand_out, contract_out)
        rep, fs, tp = lax.axis_index("rep"), lax.axis_index("fs"), lax.axis_index("tp")
        a, b = fs // inner, lax.rem(fs, inner)
        far = [lax.rem(a + d, outer) * inner + b for d in range(1, outer)]
        near = [a * inner + lax.rem(b + d, inner) for d in range(1, inner)]
        peers = [{"fs": index} for index in far + near]
        others = [
            {"rep": lax.rem(rep + i, n_rep), "tp": lax.rem(tp + j, n_tp)}
            for i in range(n_rep)
            for j in range(n_tp)
            if i or j
        ]
        barrier = pltpu.get_barrier_semaphore()
        for peer in peers + others:
            pl.semaphore_signal(barrier, inc=1, device_id=peer, device_id_type=MESH)
        pl.semaphore_wait(barrier, len(peers) + len(others))

        def block(w, start, size, index):
            across = weights[w].shape[axes[w]]
            offset = pl.multiple_of(index * across, across)
            if axes[w] == 0:
                return outs[w].at[pl.ds(offset + start, size), :]
            return outs[w].at[pl.ds(start, size), pl.ds(offset, across)]

        far_copies, near_copies, own_copies = {}, {}, {}

        def launch_far(c):
            w, start, size = chunks[c]
            source, target = sources[w].at[pl.ds(start, size), :], block(w, start, size, fs)
            far_copies[c] = [
                send_to(source, target, far_send.at[c, d], far_recv.at[c, d], {"fs": index})
                for d, index in enumerate(far)
            ]

        def launch_near(c):
            w, start, size = chunks[c]
            source, target = sources[w].at[pl.ds(start, size), :], block(w, start, size, fs)
            near_copies[c] = [
                send_to(
                    source, target, near_send.at[c, 0, e], near_recv.at[c, 0, e], {"fs": index}
                )
                for e, index in enumerate(near)
            ]
            own_copies[c] = pltpu.make_async_copy(source, target, own_sem.at[c])
            own_copies[c].start()

        def forward(c):
            w, start, size = chunks[c]
            for d in range(1, outer):
                far_copies[c][d - 1].wait_recv()
                held_block = block(w, start, size, lax.rem(a + outer - d, outer) * inner + b)
                near_copies[c] += [
                    send_to(
                        held_block,
                        held_block,
                        near_send.at[c, d, e],
                        near_recv.at[c, d, e],
                        {"fs": index},
                    )
                    for e, index in enumerate(near)
                ]

        def arrived(c):
            for copy in near_copies[c]:
                copy.wait_recv()
            own_copies[c].wait()

        first = [c for c in range(count) if chunks[c][0] == 0]
        second = [c for c in range(count) if chunks[c][0] == 1]
        later = [c for c in range(count) if chunks[c][0] > 1]

        spot = whole_ref.at[
            pl.ds(pl.multiple_of(rep * length, length), length),
            pl.ds(pl.multiple_of(tp * columns, columns), columns),
        ]
        own = pltpu.make_async_copy(features_ref, spot, own_sem.at[count])
        own.start()
        group_copies = [
            send_to(features_ref, spot, group_send.at[d], group_recv.at[d], peer)
            for d, peer in enumerate(others)
        ]
        for c in first:
            launch_far(c)
            launch_near(c)
        for c in second + later:
            launch_far(c)
        for c in first:
            forward(c)
        for c in second + later:
            launch_near(c)
        for c in first:
            arrived(c)
        own.wait()
        for copy in group_copies:
            copy.wait()

        def sequence(i, carry):
            at = pl.ds(pl.multiple_of(i * length, length), length)
            normed = row_norm(whole_ref[at, :], gain_ref[...])
            sums = jnp.dot(normed, project_out[...], preferred_element_type=F32)
            gated_ref[at, :] = attend_rows(
                sums, shift_ref[...], spike_ref[at, :], scale_ref[...], heads
            )
            return carry

        lax.fori_loop(0, n_rep, sequence, 0)
        for c in second:
            forward(c)
        waiting = list(later)
        for c in waiting[:1]:
            forward(c)
        waiting = waiting[1:]
        for c in second:
            arrived(c)
        if inside:

            def mixer(i, carry):
                at = pl.ds(pl.multiple_of(i * length, length), length)
                partial_ref[at, :] = jnp.dot(
                    gated_ref[at, :], result_out[...], preferred_element_type=F32
                ).astype(BF16)
                return carry

            lax.fori_loop(0, n_rep, mixer, 0)

            def between(stage):
                if stage in (1, 2):
                    forward(waiting.pop(0))

            reduce_steps(
                partial_ref,
                features_ref,
                middle_ref,
                mid_ref,
                slot_a,
                held,
                slot_b,
                sum_send,
                sum_recv,
                sizes,
                between,
            )
        for c in waiting:
            forward(c)
        for c in later:
            arrived(c)
        for c in range(count):
            for copy in far_copies[c] + near_copies[c]:
                copy.wait_send()

    dma = pltpu.SemaphoreType.DMA
    vmem = pl.BlockSpec(memory_space=pltpu.VMEM)
    hbm = pl.BlockSpec(memory_space=pl.ANY)
    out_shape = [jax.ShapeDtypeStruct(full[2], BF16), jax.ShapeDtypeStruct(full[3], BF16)]
    scratch = []
    gated_shape = (rows, value_lanes)
    if inside:
        out_shape += [
            jax.ShapeDtypeStruct((length, columns), BF16),
            jax.ShapeDtypeStruct((rows, columns * n_tp), BF16),
        ]
        out_specs = [hbm, hbm, vmem, vmem]
        scratch += [
            pltpu.VMEM(full[1], BF16),
            pltpu.VMEM(gated_shape, BF16),
            pltpu.VMEM((rows, columns * n_tp), BF16),
            pltpu.VMEM((max(n_tp - 1, 1), rows, columns), BF16),
            pltpu.VMEM((rows, columns), BF16),
            pltpu.VMEM((max(n_rep - 1, 1), length, columns), BF16),
        ]
    else:
        out_shape += [
            jax.ShapeDtypeStruct(full[1], BF16),
            jax.ShapeDtypeStruct(gated_shape, BF16),
        ]
        out_specs = [hbm, hbm, hbm, vmem]
    scratch += [
        pltpu.VMEM(full[0], BF16),
        pltpu.VMEM((rows, columns * n_tp), BF16),
        dma((count, max(outer - 1, 1))),
        dma((count, max(outer - 1, 1))),
        dma((count, outer, max(inner - 1, 1))),
        dma((count, outer, max(inner - 1, 1))),
        dma((count + 1,)),
        dma((group,)),
        dma((group,)),
    ]
    if inside:
        scratch += [dma((4, most)), dma((4, most))]
    return pl.pallas_call(
        kernel,
        out_shape=out_shape,
        in_specs=[vmem] * 9,
        out_specs=out_specs,
        scratch_shapes=scratch,
        compiler_params=pltpu.CompilerParams(
            collective_id=0, has_side_effects=True, vmem_limit_bytes=VMEM_LIMIT
        ),
        name="first_half",
    )(
        *weights,
        features,
        gain.reshape(1, -1),
        shift.reshape(1, -1),
        spike,
        scale.astype(F32).reshape(1, -1),
    )


def reduce_steps(
    part_ref, base_ref, out_ref, all_ref, slot_a, held, slot_b, send_sem, recv_sem, sizes, between
):
    n_rep, n_fs, n_tp = sizes
    rows, columns = base_ref.shape
    rep, tp = lax.axis_index("rep"), lax.axis_index("tp")
    tps = [lax.rem(tp + d, n_tp) for d in range(1, n_tp)]
    reps = [lax.rem(rep + d, n_rep) for d in range(1, n_rep)]

    def send(stage, d, source, target, peer):
        return send_to(source, target, send_sem.at[stage, d], recv_sem.at[stage, d], peer)

    copies = [
        send(0, d, place(part_ref, 1, index, columns), slot_a.at[d], {"tp": index})
        for d, index in enumerate(tps)
    ]
    for copy in copies:
        copy.wait()
    total = place(part_ref, 1, tp, columns)[...].astype(F32)
    for d in range(len(tps)):
        total = total + slot_a[d].astype(F32)
    held[...] = total.astype(BF16)
    copies = [
        send(1, d, place(held, 0, index, rows), slot_b.at[d], {"rep": index})
        for d, index in enumerate(reps)
    ]
    between(1)
    for copy in copies:
        copy.wait()
    total = place(held, 0, rep, rows)[...].astype(F32)
    for d in range(len(reps)):
        total = total + slot_b[d].astype(F32)
    result = (base_ref[...].astype(F32) + total.astype(BF16).astype(F32)).astype(BF16)
    out_ref[...] = result
    if all_ref is not None:
        block = all_ref.at[
            pl.ds(pl.multiple_of(rep * rows, rows), rows),
            pl.ds(pl.multiple_of(tp * columns, columns), columns),
        ]
        block[...] = result
        copies = [send(2, d, block, block, {"rep": index}) for d, index in enumerate(reps)]
        between(2)
        for copy in copies:
            copy.wait()
        strip = place(all_ref, 1, tp, columns)
        copies = [send(3, d, strip, strip, {"tp": index}) for d, index in enumerate(tps)]
        for copy in copies:
            copy.wait()


def reduce_group(partial, base, sizes, spread, collective_id):
    n_rep, n_fs, n_tp = sizes
    rows, columns = base.shape

    def kernel(*refs):
        part_ref, base_ref = refs[:2]
        if spread:
            out_ref, all_ref, slot_a, held, slot_b, send_sem, recv_sem = refs[2:]
        else:
            all_ref = None
            out_ref, slot_a, held, slot_b, send_sem, recv_sem = refs[2:]
        rep, tp = lax.axis_index("rep"), lax.axis_index("tp")
        barrier = pltpu.get_barrier_semaphore()
        for d in range(1, n_tp):
            peer = {"tp": lax.rem(tp + d, n_tp)}
            pl.semaphore_signal(barrier, inc=1, device_id=peer, device_id_type=MESH)
        for d in range(1, n_rep):
            peer = {"rep": lax.rem(rep + d, n_rep)}
            pl.semaphore_signal(barrier, inc=1, device_id=peer, device_id_type=MESH)
        pl.semaphore_wait(barrier, n_tp + n_rep - 2)
        reduce_steps(
            part_ref,
            base_ref,
            out_ref,
            all_ref,
            slot_a,
            held,
            slot_b,
            send_sem,
            recv_sem,
            sizes,
            lambda stage: None,
        )

    out_shape = [jax.ShapeDtypeStruct((rows, columns), BF16)]
    if spread:
        out_shape.append(jax.ShapeDtypeStruct((rows * n_rep, columns * n_tp), BF16))
    vmem = pl.BlockSpec(memory_space=pltpu.VMEM)
    most = max(n_rep, n_tp)
    return pl.pallas_call(
        kernel,
        out_shape=out_shape,
        in_specs=[vmem, vmem],
        out_specs=[vmem] * len(out_shape),
        scratch_shapes=[
            pltpu.VMEM((max(n_tp - 1, 1), rows * n_rep, columns), BF16),
            pltpu.VMEM((rows * n_rep, columns), BF16),
            pltpu.VMEM((max(n_rep - 1, 1), rows, columns), BF16),
            pltpu.SemaphoreType.DMA((4, most)),
            pltpu.SemaphoreType.DMA((4, most)),
        ],
        compiler_params=pltpu.CompilerParams(
            collective_id=collective_id, has_side_effects=True, vmem_limit_bytes=VMEM_LIMIT
        ),
        name="reduce_group",
    )(partial, base)


def lanes_same(shape, row_width, column_width):
    return (
        lax.broadcasted_iota(jnp.int32, shape, 0) // row_width
        == lax.broadcasted_iota(jnp.int32, shape, 1) // column_width
    ).astype(F32)


def dot32(left, right, contract=((1,), (0,))):
    return lax.dot_general(
        left, right, (contract, ((), ())), precision=HIGHEST, preferred_element_type=F32
    )


def attend_rows(sums, shift, spike, scale, heads):
    length = sums.shape[0]
    key_lanes, value_lanes = heads * HEAD_K, heads * HEAD_V

    def part(start, width):
        return sums[:, start : start + width]

    def rounded(array):
        return array.astype(BF16).astype(F32)

    query = rounded(part(0, key_lanes)) * HEAD_K ** (-0.5)
    keys = rounded(part(key_lanes, key_lanes))
    values = rounded(part(2 * key_lanes, value_lanes))
    decay_pre = part(2 * key_lanes + value_lanes, key_lanes) + shift
    gate = rounded(part(3 * key_lanes + value_lanes, value_lanes))
    log_sigmoid = jnp.minimum(decay_pre, 0.0) - jnp.log1p(jnp.exp(-jnp.abs(decay_pre)))
    c = log_sigmoid / switch_multiplier + spike
    row = lax.broadcasted_iota(jnp.int32, (length, key_lanes), 0)
    step = 1
    while step < length:
        c = c + jnp.where(row >= step, pltpu.roll(c, step, 0), 0.0)
        step *= 2

    spread = lanes_same((key_lanes, value_lanes), HEAD_K, HEAD_V)
    in_sub = lax.rem(row, SUB)
    out = dot32(query * keys, spread) * values
    for d in range(1, SUB):
        ok = in_sub >= d
        weight = jnp.exp(jnp.where(ok, c - pltpu.roll(c, d, 0), 0.0))
        product = jnp.where(ok, query * pltpu.roll(keys, d, 0) * weight, 0.0)
        out = out + dot32(product, spread) * pltpu.roll(values, d, 0)

    pieces = [jnp.zeros((SUB, value_lanes), F32)]
    stack = heads * SUB
    key_mask = lanes_same((stack, key_lanes), SUB, HEAD_K)
    value_mask = lanes_same((stack, value_lanes), SUB, HEAD_V)
    for start in range(SUB, length, SUB):
        edge = c[start - 1 : start]
        q_part = query[start : start + SUB] * jnp.exp(c[start : start + SUB] - edge)
        k_part = keys[:start] * jnp.exp(edge - c[:start])
        stacked = jnp.concatenate([q_part] * heads, axis=0) * key_mask
        scores = dot32(stacked, k_part, ((1,), (1,)))
        read = dot32(scores, values[:start]) * value_mask
        total = read[:SUB]
        for h in range(1, heads):
            total = total + read[h * SUB : (h + 1) * SUB]
        pieces.append(total)
    out = out + jnp.concatenate(pieces, axis=0)

    same = lanes_same((value_lanes, value_lanes), HEAD_V, HEAD_V)
    mean = dot32(out * out, same) / HEAD_V
    out = out * lax.rsqrt(mean + norm_eps) * scale
    return (out * (gate / (1.0 + jnp.exp(-gate)))).astype(BF16)


def causal_conv(content_tokens, taps, length):
    rows, columns = content_tokens.shape
    content_tokens = content_tokens.astype(F32).reshape(rows // length, length, columns)
    taps = taps.astype(F32)
    width = taps.shape[0]
    padded = jnp.pad(content_tokens, ((0, 0), (width - 1, 0), (0, 0)))
    total = jnp.zeros_like(content_tokens)
    for offset in range(width):
        total = total + padded[:, offset : offset + length] * taps[offset]
    return total.reshape(rows, columns)


def shards(
    sizes,
    incoming_features,
    attend_prenormal_scale,
    probe_matrix,
    lookup_matrix,
    content_matrix,
    forgetting_matrix,
    result_switch_matrix,
    forgetting_shift,
    spike_forget_logarithm,
    attend_unit_scale,
    attend_result_matrix,
    perceptron_scale,
    content_expand_matrix,
    switch_expand_matrix,
    content_kernel,
    switch_kernel,
    contract_matrix,
):
    n_rep, n_fs, n_tp = sizes
    rep = lax.axis_index("rep")
    length = incoming_features.shape[0]

    def mine(array, axis):
        size = array.shape[axis] // n_rep
        return lax.dynamic_slice_in_dim(array, rep * size, size, axis)

    project = jnp.concatenate(
        [
            mine(matrix, 1)
            for matrix in (
                probe_matrix,
                lookup_matrix,
                content_matrix,
                forgetting_matrix,
                result_switch_matrix,
            )
        ],
        axis=1,
    )
    spike_all = lax.all_to_all(
        spike_forget_logarithm, "rep", split_axis=1, concat_axis=0, tiled=True
    )
    expand = jnp.concatenate([mine(content_expand_matrix, 1), mine(switch_expand_matrix, 1)], axis=1)
    side = attend_result_matrix.shape[1]
    inside = side % 128 == 0
    outs = first_half(
        project,
        mine(attend_result_matrix, 0),
        expand,
        mine(contract_matrix, 0),
        incoming_features,
        attend_prenormal_scale,
        mine(forgetting_shift, 0),
        spike_all,
        mine(attend_unit_scale, 0),
        1 if inside else 0,
        inside,
        sizes,
    )
    if inside:
        expand_all, contract_all, middle, whole_mid = outs
    else:
        expand_all, contract_all, result_all, switched_result = outs
        result_all, contract_all = (
            array.reshape(n_fs, -1, side).swapaxes(0, 1).reshape(-1, n_fs * side)
            for array in (result_all, contract_all)
        )
        mixer_partial = jnp.dot(switched_result, result_all, preferred_element_type=F32)
        middle, whole_mid = reduce_group(
            mixer_partial.astype(BF16), incoming_features, sizes, True, 2
        )
    normed_mid = row_norm(whole_mid, perceptron_scale)
    both = jnp.dot(normed_mid, expand_all, preferred_element_type=F32).astype(BF16)
    half = both.shape[1] // 2
    conv_value = causal_conv(both[:, :half], mine(content_kernel, 1), length)
    conv_gated = causal_conv(both[:, half:], mine(switch_kernel, 1), length)
    hidden = (conv_value * jax.nn.gelu(conv_gated, approximate=True)).astype(BF16)
    down_partial = jnp.dot(hidden, contract_all, preferred_element_type=F32).astype(BF16)
    return reduce_group(down_partial, middle, sizes, False, 3)[0]


def solution(mesh):
    sizes = (mesh.shape["rep"], mesh.shape["fs"], mesh.shape["tp"])
    placed = (
        P(("rep", "fs"), "tp"),
        P(),
        P("fs", "tp"),
        P("fs", "tp"),
        P("fs", "tp"),
        P("fs", "tp"),
        P("fs", "tp"),
        P("tp"),
        P(("rep", "fs"), "tp"),
        P("tp"),
        P("tp", "fs"),
        P(),
        P("fs", "tp"),
        P("fs", "tp"),
        P(None, "tp"),
        P(None, "tp"),
        P("tp", "fs"),
    )
    return jax.shard_map(
        functools.partial(shards, sizes),
        mesh=mesh,
        in_specs=placed,
        out_specs=P(("rep", "fs"), "tp"),
        check_vma=False,
    )
```

profile of v0, /device:TPU:0, one launch (start us, length us, event | category | flops | bytes accessed | tf_op | source)
XLA Modules:
  0.0 268.8 jit_solution(2432211896326824425)
XLA Ops:
  0.0 0.0 copy-start
  0.0 0.0 copy-start.12
  0.0 0.0 copy-start.11
  0.0 0.0 copy-start.8
  0.0 0.0 copy-start.9
  0.0 0.0 copy-start.13
  0.0 0.0 copy-start.7
  0.0 0.0 copy-start.10
  0.1 0.0 copy-start.4
  0.1 1.8 copy_bitcast_fusion
  1.8 4.2 %all-to-all-start = ((f32[192,2,128]{2,0,1:T(8,128)}), f32[192,2,128]{2,0,1:T(8,128)S(1)}, u32[]{:S(2)}, u32[]{:S(2)}) async-start(f32[192,2,128]{2,0,1:T(8,128)} %copy_bitcast_fusion), calls=%async_computation | async-start | bytes 393216 | tf_op jit(solution)/shard_map/all_to_all | solution.py:542
  6.1 1.3 reshape.47.refs_5_
  7.4 0.7 convert_element_type.31
  8.0 0.0 copy-done
  8.1 0.9 constant_dynamic-slice_fusion.refs_3_
  8.9 0.0 copy-done.12
  8.9 0.0 copy-done.11
  9.0 0.0 copy-done.8
  9.0 0.0 copy-done.9
  9.0 0.0 copy-done.13
  9.0 0.7 dynamic-slice_convert_fusion.2
  9.7 0.0 copy-done.7
  9.7 0.0 copy-done.10
  9.8 0.0 copy-done.4
  9.8 1.1 constant_dynamic-slice_fusion.1
  10.9 0.0 copy-start.5
  10.9 0.0 copy-start.6
  11.0 0.0 copy-start.15
  11.0 1.1 pad_maximum_fusion.refs_2_
  12.0 0.0 copy-done.5
  12.0 0.0 copy-done.6
  12.0 0.7 dynamic-slice_dynamic-update-slice_fusion
  12.7 0.0 copy-done.15
  12.7 0.0 copy-start.3
  12.7 0.8 dynamic-slice_bitcast_fusion.refs_6_
  13.5 0.0 all-to-all-done
  13.5 0.0 copy-start.2
  13.5 0.0 copy-done.3
  13.5 0.7 copy-done.2
  14.1 221.6 %first_half.1 = (bf16[2048,2048]{1,0:T(8,128)(2,1)}, bf16[1024,2048]{1,0:T(8,128)(2,1)}, bf16[192,1024]{1,0:T(8,128)(2,1)}, bf16[384,2048]{1,0:T(8,128)(2,1)}) custom-call(bf16[256,896]{1,0:T(8,128)(2,1)} %copy-done.3, bf16[256,256]{1,0:T(8,128)(2,1)} %get-tuple-element.22.refs_1_, bf16[256,2048]{1,0:T(8,128)(2,1)} %pad_maximum_fusion.refs_2_, ...), custom_call_target="tpu_custom_call" | custom-call | tf_op jit(solution)/shard_map/first_half/pallas_call | solution.py:293
  235.8 0.0 copy-start.1
  235.8 1.9 fusion
  237.7 0.0 copy-done.1
  237.7 6.8 %convolution_convert_fusion = bf16[384,2048]{1,0:T(8,128)(2,1)S(1)} fusion(bf16[2048,2048]{1,0:T(8,128)(2,1)} %get-tuple-element.10, bf16[384,2048]{1,0:T(8,128)(2,1)S(1)} %copy-done.1, f32[2048]{0:T(1024)S(1)} %convert_element_type.31, f32[384]{0:T(512)S(1)} %add_rsqrt_fusion), kind=kOutput, calls=%fused_computation.5 | convolution fusion | flops 3225157632 | bytes 11544064 | tf_op jit(solution)/shard_map/dot_general | solution.py:575
  244.6 0.1 fusion.23
  244.7 0.2 convert.3
  244.9 0.2 convert.4
  245.0 0.5 fusion.5
  245.5 0.0 copy-start.14
  245.5 0.5 fusion.9
  246.0 0.5 fusion.19
  246.6 1.2 copy-done.14
  247.7 3.0 %convolution_convert_fusion.1.refs_0_ = bf16[384,2048]{1,0:T(8,128)(2,1)} fusion(bf16[384,1024]{1,0:T(8,128)(2,1)S(1)} %fusion.19, bf16[1024,2048]{1,0:T(8,128)(2,1)S(1)} %copy-done.14), kind=kOutput, calls=%fused_computation.6 | convolution fusion | flops 1611399168 | bytes 6553600 | tf_op jit(solution)/shard_map/dot_general | solution.py:580
  250.7 16.3 %reduce_group.1 = bf16[192,1024]{1,0:T(8,128)(2,1)} custom-call(bf16[384,2048]{1,0:T(8,128)(2,1)} %convolution_convert_fusion.1.refs_0_, bf16[192,1024]{1,0:T(8,128)(2,1)} %get-tuple-element.12.refs_1_), custom_call_target="tpu_custom_call" | custom-call | tf_op jit(solution)/shard_map/reduce_group/pallas_call | solution.py:402
  267.0 1.8 copy.26
  (8 shorter events, 0.1 us)
Async XLA Ops:
  0.0 8.0 %copy-start = (bf16[2048,256]{1,0:T(8,128)(2,1)S(1)}, bf16[2048,256]{1,0:T(8,128)(2,1)}, u32[]{:S(2)}) copy-start(bf16[2048,256]{1,0:T(8,128)(2,1)} %param.33) | copy-start | bytes 3145732
  0.0 8.9 %copy-start.12 = (bf16[3,2048]{1,0:T(4,128)(2,1)S(1)}, bf16[3,2048]{1,0:T(4,128)(2,1)}, u32[]{:S(2)}) copy-start(bf16[3,2048]{1,0:T(4,128)(2,1)} %param.31) | copy-start | bytes 36868
  0.0 8.9 %copy-start.11 = (bf16[3,2048]{1,0:T(4,128)(2,1)S(1)}, bf16[3,2048]{1,0:T(4,128)(2,1)}, u32[]{:S(2)}) copy-start(bf16[3,2048]{1,0:T(4,128)(2,1)} %param.32) | copy-start | bytes 36868
  0.0 8.9 %copy-start.8 = (bf16[256,256]{1,0:T(8,128)(2,1)S(1)}, bf16[256,256]{1,0:T(8,128)(2,1)}, u32[]{:S(2)}) copy-start(bf16[256,256]{1,0:T(8,128)(2,1)} %param.19) | copy-start | bytes 393220
  0.0 9.0 %copy-start.9 = (bf16[256,256]{1,0:T(8,128)(2,1)S(1)}, bf16[256,256]{1,0:T(8,128)(2,1)}, u32[]{:S(2)}) copy-start(bf16[256,256]{1,0:T(8,128)(2,1)} %param.20) | copy-start | bytes 393220
  0.0 9.0 %copy-start.13 = (bf16[512]{0:T(512)(128)(2,1)S(1)}, bf16[512]{0:T(512)(128)(2,1)}, u32[]{:S(2)}) copy-start(bf16[512]{0:T(512)(128)(2,1)} %param.26) | copy-start | bytes 3076
  0.0 9.7 %copy-start.7 = (bf16[256,512]{1,0:T(8,128)(2,1)S(1)}, bf16[256,512]{1,0:T(8,128)(2,1)}, u32[]{:S(2)}) copy-start(bf16[256,512]{1,0:T(8,128)(2,1)} %param.21) | copy-start | bytes 786436
  0.0 9.7 %copy-start.10 = (bf16[256,256]{1,0:T(8,128)(2,1)S(1)}, bf16[256,256]{1,0:T(8,128)(2,1)}, u32[]{:S(2)}) copy-start(bf16[256,256]{1,0:T(8,128)(2,1)} %param.22) | copy-start | bytes 393220
  0.1 9.7 %copy-start.4 = (bf16[256,2048]{1,0:T(8,128)(2,1)S(1)}, bf16[256,2048]{1,0:T(8,128)(2,1)}, u32[]{:S(2)}) copy-start(bf16[256,2048]{1,0:T(8,128)(2,1)} %param.30) | copy-start | bytes 3145732
  1.8 11.6 %all-to-all-start = ((f32[192,2,128]{2,0,1:T(8,128)}), f32[192,2,128]{2,0,1:T(8,128)S(1)}, u32[]{:S(2)}, u32[]{:S(2)}) async-start(f32[192,2,128]{2,0,1:T(8,128)} %copy_bitcast_fusion), calls=%async_computation | async-start | bytes 393216 | tf_op jit(solution)/shard_map/all_to_all | solution.py:542
  10.9 1.1 copy-start.5
  10.9 1.1 copy-start.6
  11.0 1.7 copy-start.15
  12.7 0.8 copy-start.3
  13.5 0.7 copy-start.2
  235.8 1.9 copy-start.1
  245.5 2.2 copy-start.14
where the time goes:
time: 272 us; the launch traced here: 269 us
  Pallas kernels  238 us (88%)
  local copies, waits for them, and re-layouts  10.4 us (4%)
  matrix products  9.84 us (4%)
  other arithmetic  6.14 us (2%)
  starting transfers between devices  4.24 us (2%)
    pallas_call x1, Pallas kernels, first_half(): pl.pallas_call(kernel, out_shape=out_shape, in_specs=[vmem] * 9, out_spec...  222 us
    pallas_call x1, Pallas kernels, reduce_group(): pl.pallas_call(kernel, out_shape=out_shape, in_specs=[vmem, vmem], out_sp...  16.3 us
    dot_general x1, matrix products, shards(): jnp.dot(normed_mid, expand_all, preferred_element_type=F32).astype(BF16)  6.84 us
  transfers between devices with their start and end apart: 1, of which 0 were waited for; matrix products, arithmetic and copies ran while one was open for 3% of the time, Pallas kernels for 0%

commit v1 on v0

--- a/solution.py
+++ b/solution.py
@@ -16,7 +16,6 @@
 MESH = pl.DeviceIdType.MESH
 F32 = jnp.float32
 BF16 = jnp.bfloat16
-HIGHEST = lax.Precision.HIGHEST
 VMEM_LIMIT = 60 * 1024 * 1024
 
 
@@ -427,7 +426,7 @@
 
 def dot32(left, right, contract=((1,), (0,))):
     return lax.dot_general(
-        left, right, (contract, ((), ())), precision=HIGHEST, preferred_element_type=F32
+        left.astype(BF16), right.astype(BF16), (contract, ((), ())), preferred_element_type=F32
     )
 
 
@@ -496,6 +495,515 @@
     for offset in range(width):
         total = total + padded[:, offset : offset + length] * taps[offset]
     return total.reshape(rows, columns)
+
+
+def pair_size(outer):
+    return 2 if outer % 2 == 0 else 1
+
+
+def fits(sizes, features, probe, result, content):
+    n_rep, n_fs, n_tp = sizes
+    outer, inner = factor(n_fs)
+    members = n_rep * pair_size(outer)
+    return (
+        features.shape[0] % 16 == 0
+        and features.shape[1] % 128 == 0
+        and probe.shape[1] % (128 * n_rep) == 0
+        and result.shape[1] % 128 == 0
+        and result.shape[0] % (128 * n_rep) == 0
+        and content.shape[1] % (128 * members) == 0
+        and outer & (outer - 1) == 0
+        and outer % n_tp == 0
+    )
+
+
+def partner(a, d, outer):
+    total, bit = 0, 1
+    while bit < outer:
+        total = total + lax.rem(a // bit + (d // bit) % 2, 2) * bit
+        bit *= 2
+    return total
+
+
+def shifted(array, step, row):
+    return jnp.where(row >= step, pltpu.roll(array, step, 0), 0.0)
+
+
+def taps_sum(array, taps):
+    taps = taps.astype(F32)
+    width = taps.shape[0]
+    row = lax.broadcasted_iota(jnp.int32, array.shape, 0)
+    total = jnp.zeros_like(array)
+    for offset in range(width):
+        back = width - 1 - offset
+        moved = array if back == 0 else shifted(array, back, row)
+        total = total + moved * taps[offset : offset + 1]
+    return total
+
+
+def whole_layer(
+    sizes,
+    features,
+    first_gain,
+    weights,
+    shift,
+    spike,
+    scale,
+    second_gain,
+    content_taps,
+    switch_taps,
+):
+    n_rep, n_fs, n_tp = sizes
+    outer, inner = factor(n_fs)
+    n_pair = pair_size(outer)
+    members = n_rep * n_pair
+    length, columns = features.shape
+    wide = columns * n_tp
+    rows = length * n_rep
+    tokens = length * members
+    key_lanes = weights[0].shape[1] // n_rep
+    heads = key_lanes // HEAD_K
+    value_lanes = heads * HEAD_V
+    units = weights[6].shape[1] // members
+    side = weights[5].shape[1]
+    runs = outer // n_tp
+
+    across = [weight.shape[0] for weight in weights[:5]] + [side]
+    across += [weights[6].shape[0], weights[7].shape[0], side]
+    kinds = ("project",) * 5 + ("result", "expand", "expand", "contract")
+    widths = [weight.shape[1] // n_rep for weight in weights[:5]]
+    offsets = [sum(widths[:w]) for w in range(5)]
+    part_rows = {5: weights[5].shape[0] // n_rep, 8: weights[8].shape[0] // members}
+    chunks = [(w, 0, weights[w].shape[0]) for w in range(5)] + [(5, 0, part_rows[5])]
+    split = pieces_of(weights[6].shape[0], 2)
+    size = weights[6].shape[0] // split
+    chunks += [(w, k * size, size) for k in range(split) for w in (6, 7)]
+    split = pieces_of(part_rows[8], 2)
+    size = part_rows[8] // split
+    chunks += [(8, k * size, size) for k in range(split)]
+    count = len(chunks)
+
+    def kernel(*refs):
+        sources = refs[:9]
+        (features_ref, gain_ref, shift_ref, spike_ref, scale_ref) = refs[9:14]
+        (second_ref, content_taps_ref, switch_taps_ref, out_ref) = refs[14:18]
+        (project_all, result_all, expand_all, contract_all) = refs[18:22]
+        (whole_ref, normed_ref, spike_all, gated_ref, stage, slot_a, held, slot_b) = refs[22:30]
+        (mid_all, normed_mid, hidden_ref, down_stage, slot_d, own_part, held_down, slot_c) = refs[
+            30:38
+        ]
+        (far_send, far_recv, near_send, near_recv, own_sem) = refs[38:43]
+        (group_send, group_recv, spike_send, spike_recv) = refs[43:47]
+        (mix_send, mix_recv, cross_send, cross_recv) = refs[47:51]
+        (mid_send, mid_recv, strip_send, strip_recv) = refs[51:55]
+        (down_send, down_recv, back_send, back_recv) = refs[55:59]
+        rep, fs, tp = lax.axis_index("rep"), lax.axis_index("fs"), lax.axis_index("tp")
+        a, b = fs // inner, lax.rem(fs, inner)
+        p = lax.rem(a, n_pair)
+        far = [partner(a, d, outer) for d in range(1, outer)]
+        near = [a * inner + lax.rem(b + d, inner) for d in range(1, inner)]
+        tps = [lax.rem(tp + d, n_tp) for d in range(1, n_tp)]
+        reps = [lax.rem(rep + d, n_rep) for d in range(1, n_rep)]
+        group = [
+            {"rep": lax.rem(rep + i, n_rep), "tp": lax.rem(tp + j, n_tp)}
+            for i in range(n_rep)
+            for j in range(n_tp)
+            if i or j
+        ]
+        team = []
+        senders = []
+        diagonal = []
+        for i in range(n_rep):
+            for j in range(n_pair):
+                if i or j:
+                    r, q = lax.rem(rep + i, n_rep), lax.rem(p + j, n_pair)
+                    peer = {"rep": r, "fs": (a - p + q) * inner + b}
+                    team.append((peer, r * n_pair + q))
+                    r, q = lax.rem(rep + n_rep - i, n_rep), lax.rem(p + n_pair - j, n_pair)
+                    senders.append(r * n_pair + q)
+                    if i and j:
+                        diagonal.append(peer)
+        me = rep * n_pair + p
+        greeted = [{"fs": index * inner + b} for index in far]
+        greeted += [{"fs": index} for index in near] + group + diagonal
+        barrier = pltpu.get_barrier_semaphore()
+        for peer in greeted:
+            pl.semaphore_signal(barrier, inc=1, device_id=peer, device_id_type=MESH)
+        pl.semaphore_wait(barrier, len(greeted))
+
+        def at(start, size):
+            return pl.ds(pl.multiple_of(start, size), size)
+
+        def source(c, position):
+            w, start, size = chunks[c]
+            member = rep * n_pair + lax.rem(position, n_pair)
+            if kinds[w] == "project":
+                return sources[w].at[pl.ds(start, size), at(rep * widths[w], widths[w])]
+            if kinds[w] == "expand":
+                return sources[w].at[pl.ds(start, size), at(member * units, units)]
+            index = rep if kinds[w] == "result" else member
+            base = pl.multiple_of(index * part_rows[w], part_rows[w])
+            return sources[w].at[pl.ds(base + start, size), :]
+
+        def block(c, index):
+            w, start, size = chunks[c]
+            base = pl.multiple_of(index * across[w], across[w])
+            if kinds[w] == "project":
+                return project_all.at[pl.ds(base + start, size), pl.ds(offsets[w], widths[w])]
+            if kinds[w] == "expand":
+                return expand_all.at[pl.ds(base + start, size), pl.ds((w - 6) * units, units)]
+            target = result_all if kinds[w] == "result" else contract_all
+            return target.at[pl.ds(start, size), pl.ds(base, across[w])]
+
+        sent = []
+        far_copies, near_copies, own_copies = {}, {}, {}
+
+        def launch_far(c):
+            far_copies[c] = [
+                send_to(
+                    source(c, position),
+                    block(c, fs),
+                    far_send.at[c, d],
+                    far_recv.at[c, d],
+                    {"fs": position * inner + b},
+                )
+                for d, position in enumerate(far)
+            ]
+            sent.extend(far_copies[c])
+
+        def launch_near(c):
+            near_copies[c] = [
+                send_to(
+                    source(c, a),
+                    block(c, fs),
+                    near_send.at[c, 0, e],
+                    near_recv.at[c, 0, e],
+                    {"fs": index},
+                )
+                for e, index in enumerate(near)
+            ]
+            sent.extend(near_copies[c])
+            own_copies[c] = pltpu.make_async_copy(source(c, a), block(c, fs), own_sem.at[c])
+            own_copies[c].start()
+
+        def forward(c):
+            for d, position in enumerate(far):
+                far_copies[c][d].wait_recv()
+                landed = block(c, position * inner + b)
+                copies = [
+                    send_to(
+                        landed,
+                        landed,
+                        near_send.at[c, d + 1, e],
+                        near_recv.at[c, d + 1, e],
+                        {"fs": index},
+                    )
+                    for e, index in enumerate(near)
+                ]
+                near_copies[c] += copies
+                sent.extend(copies)
+
+        def arrived(c):
+            for copy in near_copies[c]:
+                copy.wait_recv()
+            own_copies[c].wait()
+
+        first = [c for c in range(count) if kinds[chunks[c][0]] == "project"]
+        second = [c for c in range(count) if kinds[chunks[c][0]] == "result"]
+        third = [c for c in range(count) if kinds[chunks[c][0]] == "expand"]
+        fourth = [c for c in range(count) if kinds[chunks[c][0]] == "contract"]
+
+        spot = whole_ref.at[at(rep * length, length), at(tp * columns, columns)]
+        own_features = pltpu.make_async_copy(features_ref, spot, own_sem.at[count])
+        own_features.start()
+        group_copies = [
+            send_to(features_ref, spot, group_send.at[d], group_recv.at[d], peer)
+            for d, peer in enumerate(group)
+        ]
+        lines = spike_all.at[at(rep * length, length), :]
+        own_spike = pltpu.make_async_copy(
+            spike_ref.at[:, at(rep * key_lanes, key_lanes)], lines, own_sem.at[count + 1]
+        )
+        own_spike.start()
+        group_copies += [
+            send_to(
+                spike_ref.at[:, at(index * key_lanes, key_lanes)],
+                lines,
+                spike_send.at[d],
+                spike_recv.at[d],
+                {"rep": index},
+            )
+            for d, index in enumerate(reps)
+        ]
+        for c in first:
+            launch_far(c)
+            launch_near(c)
+        for c in second + third:
+            launch_far(c)
+        own_features.wait()
+        own_spike.wait()
+        for copy in group_copies:
+            copy.wait()
+
+        def first_norm(i, carry):
+            lines = at(i * length, length)
+            normed_ref[lines, :] = row_norm(whole_ref[lines, :], gain_ref[...])
+            return carry
+
+        lax.fori_loop(0, n_rep, first_norm, 0)
+        for c in first:
+            forward(c)
+        half = len(third) // 2
+        for c in second + third[:half]:
+            launch_near(c)
+        for c in first:
+            arrived(c)
+
+        def attention(index):
+            lines = at(index * length, length)
+            sums = jnp.dot(normed_ref[lines, :], project_all[...], preferred_element_type=F32)
+            gated_ref[lines, :] = attend_rows(
+                sums,
+                shift_ref[:, at(rep * key_lanes, key_lanes)],
+                spike_all[lines, :],
+                scale_ref[:, at(rep * value_lanes, value_lanes)].astype(F32),
+                heads,
+            )
+
+        order = reps + [rep]
+        attention(order[0])
+        for c in second:
+            forward(c)
+        for c in third[half:]:
+            launch_near(c)
+        for index in order[1:]:
+            attention(index)
+        for c in third[:half]:
+            forward(c)
+        for c in second:
+            arrived(c)
+
+        def mixed(index, strip):
+            return jnp.dot(
+                gated_ref[at(index * length, length), :],
+                result_all[:, at(strip * columns, columns)],
+                preferred_element_type=F32,
+            )
+
+        mix_copies = []
+        for i, index in enumerate(order):
+            copies = []
+            for d, other in enumerate(tps):
+                stage[i, d] = mixed(index, other).astype(BF16)
+                copies.append(
+                    send_to(
+                        stage.at[i, d],
+                        slot_a.at[i, d],
+                        mix_send.at[i, d],
+                        mix_recv.at[i, d],
+                        {"tp": other},
+                    )
+                )
+            mix_copies.append(copies)
+            sent.extend(copies)
+        cross_copies = []
+        for i, index in enumerate(order):
+            total = mixed(index, tp)
+            for d, copy in enumerate(mix_copies[i]):
+                copy.wait_recv()
+                total = total + slot_a[i, d].astype(F32)
+            if i < n_rep - 1:
+                held[i] = total.astype(BF16)
+                copy = send_to(
+                    held.at[i],
+                    slot_b.at[i],
+                    cross_send.at[i],
+                    cross_recv.at[i],
+                    {"rep": index},
+                )
+                cross_copies.append(copy)
+                sent.append(copy)
+            else:
+                for d, copy in enumerate(cross_copies):
+                    copy.wait_recv()
+                    total = total + slot_b[d].astype(F32)
+        base = whole_ref[at(rep * length, length), at(tp * columns, columns)].astype(F32)
+        mine = mid_all.at[at(me * length, length), at(tp * columns, columns)]
+        mine[...] = (base + total.astype(BF16).astype(F32)).astype(BF16)
+
+        mid_copies = [
+            send_to(mine, mine, mid_send.at[k], mid_recv.at[k], peer)
+            for k, (peer, member) in enumerate(team)
+        ]
+        sent.extend(mid_copies)
+        strip_copies = []
+
+        def strips(k, member):
+            strip = mid_all.at[at(member * length, length), at(tp * columns, columns)]
+            copies = [
+                send_to(
+                    strip, strip, strip_send.at[k, d], strip_recv.at[k, d], {"tp": index}
+                )
+                for d, index in enumerate(tps)
+            ]
+            strip_copies.append(copies)
+            sent.extend(copies)
+
+        strips(0, me)
+        for c in fourth:
+            launch_far(c)
+        for c in third[half:]:
+            forward(c)
+        for c in fourth:
+            launch_near(c)
+        for k, member in enumerate(senders):
+            mid_copies[k].wait_recv()
+            strips(k + 1, member)
+
+        def second_norm(member):
+            lines = at(member * length, length)
+            normed_mid[lines, :] = row_norm(mid_all[lines, :], second_ref[...])
+
+        for k, member in enumerate([me] + senders):
+            for copy in strip_copies[k]:
+                copy.wait_recv()
+            second_norm(member)
+        for c in third:
+            arrived(c)
+
+        def expand(i, carry):
+            lines = at(i * length, length)
+            both = jnp.dot(normed_mid[lines, :], expand_all[...], preferred_element_type=F32)
+            both = both.astype(BF16).astype(F32)
+            value = taps_sum(both[:, :units], content_taps_ref[:, at(me * units, units)])
+            gate = taps_sum(both[:, units:], switch_taps_ref[:, at(me * units, units)])
+            hidden_ref[lines, :] = (value * jax.nn.gelu(gate, approximate=True)).astype(BF16)
+            return carry
+
+        lax.fori_loop(0, members, expand, 0)
+        for c in fourth:
+            forward(c)
+
+        back_copies = []
+        for e in range(inner):
+            lane = lax.rem(b + inner - e, inner)
+            for c in fourth:
+                if e == 0:
+                    own_copies[c].wait()
+                else:
+                    for d in range(outer):
+                        near_copies[c][d * (inner - 1) + e - 1].wait_recv()
+            spots = [at((run * inner + lane) * side, side) for run in range(runs)]
+
+            def product(strip, run):
+                index = (strip * runs + run) * inner + lane
+                return jnp.dot(
+                    hidden_ref[...],
+                    contract_all[:, at(index * side, side)],
+                    preferred_element_type=F32,
+                )
+
+            down_copies = []
+            for run in range(runs):
+                copies = []
+                for d, other in enumerate(tps):
+                    down_stage[d, :, spots[run]] = product(other, run).astype(BF16)
+                    copies.append(
+                        send_to(
+                            down_stage.at[d, :, spots[run]],
+                            slot_d.at[d, :, spots[run]],
+                            down_send.at[e, run, d],
+                            down_recv.at[e, run, d],
+                            {"tp": other},
+                        )
+                    )
+                down_copies.append(copies)
+                sent.extend(copies)
+            for run in range(runs):
+                total = product(tp, run)
+                for d, copy in enumerate(down_copies[run]):
+                    copy.wait_recv()
+                    total = total + slot_d[d, :, spots[run]].astype(F32)
+                own_part[:, spots[run]] = total
+                held_down[:, spots[run]] = total.astype(BF16)
+                for k, (peer, member) in enumerate(team):
+                    copy = send_to(
+                        held_down.at[at(member * length, length), spots[run]],
+                        slot_c.at[k, :, spots[run]],
+                        back_send.at[e, run, k],
+                        back_recv.at[e, run, k],
+                        peer,
+                    )
+                    back_copies.append(copy)
+        for copy in back_copies:
+            copy.wait_recv()
+        total = own_part[at(me * length, length), :]
+        for k in range(members - 1):
+            total = total + slot_c[k].astype(F32)
+        out_ref[...] = (mine[...].astype(F32) + total.astype(BF16).astype(F32)).astype(BF16)
+        for copy in sent + back_copies:
+            copy.wait_send()
+
+    dma = pltpu.SemaphoreType.DMA
+    vmem = pl.BlockSpec(memory_space=pltpu.VMEM)
+    hbm = pl.BlockSpec(memory_space=pl.ANY)
+
+    def pair(*shape):
+        shape = tuple(max(n, 1) for n in shape)
+        return [dma(shape), dma(shape)]
+
+    def room(*shape, dtype=BF16):
+        return pltpu.VMEM(tuple(max(n, 1) for n in shape), dtype)
+
+    depth = weights[0].shape[0] * n_fs
+    scratch = [
+        room(depth, sum(widths)),
+        room(part_rows[5], side * n_fs),
+        room(depth, 2 * units),
+        room(part_rows[8], side * n_fs),
+        room(rows, wide),
+        room(rows, wide),
+        room(rows, key_lanes, dtype=F32),
+        room(rows, value_lanes),
+        room(n_rep, n_tp - 1, length, columns),
+        room(n_rep, n_tp - 1, length, columns),
+        room(n_rep - 1, length, columns),
+        room(n_rep - 1, length, columns),
+        room(tokens, wide),
+        room(tokens, wide),
+        room(tokens, units),
+        room(n_tp - 1, tokens, columns),
+        room(n_tp - 1, tokens, columns),
+        room(tokens, columns, dtype=F32),
+        room(tokens, columns),
+        room(members - 1, length, columns),
+    ]
+    scratch += pair(count, outer - 1) + pair(count, outer, inner - 1) + [dma((count + 2,))]
+    scratch += pair(n_rep * n_tp - 1) + pair(n_rep - 1)
+    scratch += pair(n_rep, n_tp - 1) + pair(n_rep - 1)
+    scratch += pair(members - 1) + pair(members, n_tp - 1)
+    scratch += pair(inner, runs, n_tp - 1) + pair(inner, runs, members - 1)
+    return pl.pallas_call(
+        kernel,
+        out_shape=jax.ShapeDtypeStruct((length, columns), BF16),
+        in_specs=[hbm] * 10 + [vmem] * 7,
+        out_specs=vmem,
+        scratch_shapes=scratch,
+        compiler_params=pltpu.CompilerParams(
+            collective_id=0, has_side_effects=True, vmem_limit_bytes=VMEM_LIMIT
+        ),
+        name="whole_layer",
+    )(
+        *weights,
+        features,
+        first_gain.reshape(1, -1),
+        shift.reshape(1, -1),
+        spike,
+        scale.reshape(1, -1),
+        second_gain.reshape(1, -1),
+        content_taps,
+        switch_taps,
+    )
 
 
 def shards(
@@ -521,6 +1029,31 @@
     n_rep, n_fs, n_tp = sizes
     rep = lax.axis_index("rep")
     length = incoming_features.shape[0]
+    if fits(
+        sizes, incoming_features, probe_matrix, attend_result_matrix, content_expand_matrix
+    ):
+        return whole_layer(
+            sizes,
+            incoming_features,
+            attend_prenormal_scale,
+            (
+                probe_matrix,
+                lookup_matrix,
+                content_matrix,
+                forgetting_matrix,
+                result_switch_matrix,
+                attend_result_matrix,
+                content_expand_matrix,
+                switch_expand_matrix,
+                contract_matrix,
+            ),
+            forgetting_shift,
+            spike_forget_logarithm,
+            attend_unit_scale,
+            perceptron_scale,
+            content_kernel,
+            switch_kernel,
+        )
 
     def mine(array, axis):
         size = array.shape[axis] // n_rep

time: 272 us -> 179 us (0.66)
  Pallas kernels: 238 us -> 174 us
  matrix products: 9.84 us -> 0 us
  other arithmetic: 6.14 us -> 0 us
  local copies, waits for them, and re-layouts: 10.4 us -> 4.34 us
  starting transfers between devices: 4.24 us -> 0 us
    pallas_call x2 -> x1, Pallas kernels: 238 us -> 174 us  [whole_layer(): pl.pallas_call(kernel, out_shape=jax.ShapeDtypeStruct((length, columns),...]
    dot_general x2 -> x0, matrix products: 9.84 us -> none  [the longest x1 6.84 us: shards(): jnp.dot(normed_mid, expand_all, preferred_element_type=F32).astype(BF16)]
    all_to_all x1 -> x0, starting transfers between devices: 4.24 us -> none  [shards(): lax.all_to_all(spike_forget_logarithm, 'rep', split_axis=1, concat_axis=0...]
  transfers between devices with their start and end apart: 1 -> 0, of which waited for: 0 -> 0; matrix products, arithmetic and copies ran while one was open for 3% -> 0% of each run, Pallas kernels for 0% -> 0%
where the time goes in v1:
time: 179 us; the launch traced here: 178 us
  Pallas kernels  174 us (97%)
  local copies, waits for them, and re-layouts  4.34 us (2%)
    pallas_call x1, Pallas kernels, whole_layer(): pl.pallas_call(kernel, out_shape=jax.ShapeDtypeStruct((length, columns),...  174 us

profile of v1, /device:TPU:0, one launch (start us, length us, event | category | flops | bytes accessed | tf_op | source)
XLA Modules:
  0.0 178.5 jit_solution(16231278638117210666)
XLA Ops:
  0.0 0.0 copy-start
  0.0 1.3 reshape.14.refs_13_
  1.3 0.0 copy-done
  1.3 0.0 copy-start.1
  1.3 0.6 reshape.12.refs_10_
  1.9 0.1 copy-done.1
  2.0 0.6 reshape.15.refs_14_
  2.6 174.1 %whole_layer.1 = bf16[192,1024]{1,0:T(8,128)(2,1)} custom-call(bf16[256,256]{1,0:T(8,128)(2,1)} %refs_0_.1, bf16[256,256]{1,0:T(8,128)(2,1)} %refs_1_.1, bf16[256,512]{1,0:T(8,128)(2,1)} %refs_2_.1, bf16[256,256]{1,0:T(8,128)(2,1)} %refs_3_.1, bf16[256,512]{1,0:T(8,128)(2,1)} %refs_4_.1, bf16[512,256]{1,0:T(8,128)(2,1)} %refs_5_.1, ...), custom_call_target="tpu_custom_call" | custom-call | tf_op jit(solution)/shard_map/whole_layer/pallas_call | solution.py:986
  176.7 1.8 copy.19
Async XLA Ops:
  0.0 1.3 copy-start
  1.3 0.7 copy-start.1

commit v2 on v1

--- a/solution.py
+++ b/solution.py
@@ -508,11 +508,13 @@
     return (
         features.shape[0] % 16 == 0
         and features.shape[1] % 128 == 0
-        and probe.shape[1] % (128 * n_rep) == 0
+        and probe.shape[0] % (16 * n_rep) == 0
+        and probe.shape[1] % (128 * inner) == 0
         and result.shape[1] % 128 == 0
-        and result.shape[0] % (128 * n_rep) == 0
+        and result.shape[0] % (128 * inner * n_rep) == 0
         and content.shape[1] % (128 * members) == 0
         and outer & (outer - 1) == 0
+        and members == 2 * n_rep
         and outer % n_tp == 0
     )
 
@@ -559,27 +561,27 @@
     members = n_rep * n_pair
     length, columns = features.shape
     wide = columns * n_tp
-    rows = length * n_rep
+    rows = length * inner
     tokens = length * members
-    key_lanes = weights[0].shape[1] // n_rep
+    key_lanes = weights[0].shape[1] // inner
     heads = key_lanes // HEAD_K
     value_lanes = heads * HEAD_V
     units = weights[6].shape[1] // members
     side = weights[5].shape[1]
     runs = outer // n_tp
-
-    across = [weight.shape[0] for weight in weights[:5]] + [side]
-    across += [weights[6].shape[0], weights[7].shape[0], side]
-    kinds = ("project",) * 5 + ("result", "expand", "expand", "contract")
-    widths = [weight.shape[1] // n_rep for weight in weights[:5]]
+    aligned = runs == n_pair
+    pieces = pieces_of(length, 2)
+
+    firsts = (0, 1, 3, 2, 4, 5)
+    widths = [weights[w].shape[1] // inner for w in range(5)]
     offsets = [sum(widths[:w]) for w in range(5)]
-    part_rows = {5: weights[5].shape[0] // n_rep, 8: weights[8].shape[0] // members}
-    chunks = [(w, 0, weights[w].shape[0]) for w in range(5)] + [(5, 0, part_rows[5])]
-    split = pieces_of(weights[6].shape[0], 2)
-    size = weights[6].shape[0] // split
-    chunks += [(w, k * size, size) for k in range(split) for w in (6, 7)]
-    split = pieces_of(part_rows[8], 2)
-    size = part_rows[8] // split
+    shard = weights[0].shape[0]
+    result_rows = weights[5].shape[0] // inner
+    down_rows = weights[8].shape[0] // members
+    split = pieces_of(shard, 2)
+    chunks = [(w, k * (shard // split), shard // split) for k in range(split) for w in (6, 7)]
+    split = pieces_of(down_rows, 2)
+    size = down_rows // split
     chunks += [(8, k * size, size) for k in range(split)]
     count = len(chunks)
 
@@ -593,10 +595,11 @@
             30:38
         ]
         (far_send, far_recv, near_send, near_recv, own_sem) = refs[38:43]
-        (group_send, group_recv, spike_send, spike_recv) = refs[43:47]
-        (mix_send, mix_recv, cross_send, cross_recv) = refs[47:51]
-        (mid_send, mid_recv, strip_send, strip_recv) = refs[51:55]
-        (down_send, down_recv, back_send, back_recv) = refs[55:59]
+        (spike_send, spike_recv, mix_send, mix_recv, cross_send, cross_recv) = refs[43:49]
+        (group_send, group_recv, y_send, y_recv, z_send, z_recv) = refs[49:55]
+        second_spread = refs[55:61]
+        (down_send, down_recv, back_send, back_recv, pass_send, held_twin) = refs[61:67]
+        (x_send, x_recv, first_sem) = refs[67:70]
         rep, fs, tp = lax.axis_index("rep"), lax.axis_index("fs"), lax.axis_index("tp")
         a, b = fs // inner, lax.rem(fs, inner)
         p = lax.rem(a, n_pair)
@@ -604,14 +607,14 @@
         near = [a * inner + lax.rem(b + d, inner) for d in range(1, inner)]
         tps = [lax.rem(tp + d, n_tp) for d in range(1, n_tp)]
         reps = [lax.rem(rep + d, n_rep) for d in range(1, n_rep)]
+        sides = [lax.rem(b + d, inner) for d in range(1, inner)]
         group = [
-            {"rep": lax.rem(rep + i, n_rep), "tp": lax.rem(tp + j, n_tp)}
-            for i in range(n_rep)
+            {"fs": a * inner + lax.rem(b + i, inner), "tp": lax.rem(tp + j, n_tp)}
+            for i in range(inner)
             for j in range(n_tp)
             if i or j
         ]
         team = []
-        senders = []
         diagonal = []
         for i in range(n_rep):
             for j in range(n_pair):
@@ -619,13 +622,14 @@
                     r, q = lax.rem(rep + i, n_rep), lax.rem(p + j, n_pair)
                     peer = {"rep": r, "fs": (a - p + q) * inner + b}
                     team.append((peer, r * n_pair + q))
-                    r, q = lax.rem(rep + n_rep - i, n_rep), lax.rem(p + n_pair - j, n_pair)
-                    senders.append(r * n_pair + q)
                     if i and j:
                         diagonal.append(peer)
         me = rep * n_pair + p
+        twin = rep * n_pair + lax.rem(p + 1, n_pair)
+        twin_peer = {"fs": (a - p + lax.rem(p + 1, n_pair)) * inner + b}
+        between = lax.rem(a + 1, outer) // 2 == 1
         greeted = [{"fs": index * inner + b} for index in far]
-        greeted += [{"fs": index} for index in near] + group + diagonal
+        greeted += group + diagonal + [{"rep": index} for index in reps]
         barrier = pltpu.get_barrier_semaphore()
         for peer in greeted:
             pl.semaphore_signal(barrier, inc=1, device_id=peer, device_id_type=MESH)
@@ -637,39 +641,69 @@
         def source(c, position):
             w, start, size = chunks[c]
             member = rep * n_pair + lax.rem(position, n_pair)
-            if kinds[w] == "project":
-                return sources[w].at[pl.ds(start, size), at(rep * widths[w], widths[w])]
-            if kinds[w] == "expand":
+            if w < 8:
                 return sources[w].at[pl.ds(start, size), at(member * units, units)]
-            index = rep if kinds[w] == "result" else member
-            base = pl.multiple_of(index * part_rows[w], part_rows[w])
+            base = pl.multiple_of(member * down_rows, down_rows)
             return sources[w].at[pl.ds(base + start, size), :]
 
         def block(c, index):
             w, start, size = chunks[c]
-            base = pl.multiple_of(index * across[w], across[w])
-            if kinds[w] == "project":
-                return project_all.at[pl.ds(base + start, size), pl.ds(offsets[w], widths[w])]
-            if kinds[w] == "expand":
+            if w < 8:
+                base = pl.multiple_of(index * shard, shard)
                 return expand_all.at[pl.ds(base + start, size), pl.ds((w - 6) * units, units)]
-            target = result_all if kinds[w] == "result" else contract_all
-            return target.at[pl.ds(start, size), pl.ds(base, across[w])]
-
-        sent = []
-        far_copies, near_copies, own_copies = {}, {}, {}
-
-        def launch_far(c):
-            far_copies[c] = [
-                send_to(
-                    source(c, position),
-                    block(c, fs),
-                    far_send.at[c, d],
-                    far_recv.at[c, d],
-                    {"fs": position * inner + b},
-                )
-                for d, position in enumerate(far)
-            ]
-            sent.extend(far_copies[c])
+            return contract_all.at[pl.ds(start, size), at(index * side, side)]
+
+        def origin(k, lanes_of, planes=n_rep):
+            w = firsts[k]
+            size = (result_rows if w == 5 else shard) // planes
+            start = rep * size if planes > 1 else 0
+            if w == 5:
+                return sources[w].at[at(lanes_of * result_rows + start, size), :]
+            return sources[w].at[at(start, size), at(lanes_of * widths[w], widths[w])]
+
+        def landing(k, index, planes=n_rep):
+            w = firsts[k]
+            size = (result_rows if w == 5 else shard) // planes
+            start = rep * size if planes > 1 else 0
+            if w == 5:
+                return result_all.at[at(start, size), at(index * side, side)]
+            return project_all.at[at(index * shard + start, size), pl.ds(offsets[w], widths[w])]
+
+        sent, passed = [], []
+        near_copies, own_copies = {}, {}
+
+        def send_far(c, d, slot, position):
+            copy = send_to(
+                source(c, position),
+                block(c, fs),
+                far_send.at[c, d],
+                far_recv.at[c, slot],
+                {"fs": position * inner + b},
+            )
+            sent.append(copy)
+
+        def launch_far(c, steps):
+            for d in steps:
+                send_far(c, d, d, far[d])
+
+        def launch_middle(c):
+            send_far(c, 1, jnp.where(between, 2, 1), jnp.where(between, far[2], far[1]))
+
+        def launch_end(c):
+            send_far(c, 2, jnp.where(between, 1, 2), jnp.where(between, far[1], far[2]))
+            send_far(c, 0, 0, far[0])
+
+        def landed_far(c, d):
+            landed = block(c, far[d] * inner + b)
+            pltpu.make_async_remote_copy(
+                src_ref=landed,
+                dst_ref=landed,
+                send_sem=far_send.at[c, d],
+                recv_sem=far_recv.at[c, d],
+                device_id={"fs": far[d] * inner + b},
+                device_id_type=MESH,
+            ).wait_recv()
+            return landed
 
         def launch_near(c):
             near_copies[c] = [
@@ -687,9 +721,8 @@
             own_copies[c].start()
 
         def forward(c):
-            for d, position in enumerate(far):
-                far_copies[c][d].wait_recv()
-                landed = block(c, position * inner + b)
+            for d in range(outer - 1):
+                landed = landed_far(c, d)
                 copies = [
                     send_to(
                         landed,
@@ -708,21 +741,176 @@
                 copy.wait_recv()
             own_copies[c].wait()
 
-        first = [c for c in range(count) if kinds[chunks[c][0]] == "project"]
-        second = [c for c in range(count) if kinds[chunks[c][0]] == "result"]
-        third = [c for c in range(count) if kinds[chunks[c][0]] == "expand"]
-        fourth = [c for c in range(count) if kinds[chunks[c][0]] == "contract"]
-
-        spot = whole_ref.at[at(rep * length, length), at(tp * columns, columns)]
+        third = [c for c in range(count) if chunks[c][0] < 8]
+        fourth = [c for c in range(count) if chunks[c][0] == 8]
+        relayed = outer == 4
+        every = range(outer - 1)
+
+        parts = [(h * (length // pieces), length // pieces) for h in range(pieces)]
+
+        def spread(ref, sems):
+            pair_send, pair_recv, across_send, across_recv, strip_send, strip_recv = sems
+            pair_copies, across_copies, strip_copies = {}, {}, []
+
+            def rows_of(member, h):
+                start, size = parts[h]
+                base = pl.multiple_of(member * length, length)
+                return ref.at[pl.ds(base + start, size), at(tp * columns, columns)]
+
+            def across(j, h):
+                member = rep * n_pair + lax.rem(p + n_pair - j, n_pair)
+                for i, index in enumerate(reps):
+                    copy = send_to(
+                        rows_of(member, h),
+                        rows_of(member, h),
+                        across_send.at[i, j, h],
+                        across_recv.at[i, j, h],
+                        {"rep": index},
+                    )
+                    across_copies[i, j, h] = copy
+                    sent.append(copy)
+
+            def strips(member):
+                strip = ref.at[at(member * length, length), at(tp * columns, columns)]
+                k = len(strip_copies)
+                copies = [
+                    send_to(strip, strip, strip_send.at[k, d], strip_recv.at[k, d], {"tp": index})
+                    for d, index in enumerate(tps)
+                ]
+                strip_copies.append((member, copies))
+                sent.extend(copies)
+
+            def begin():
+                for h in range(pieces):
+                    for j in range(1, n_pair):
+                        index = (a - p + lax.rem(p + j, n_pair)) * inner + b
+                        copy = send_to(
+                            rows_of(me, h),
+                            rows_of(me, h),
+                            pair_send.at[j - 1, h],
+                            pair_recv.at[j - 1, h],
+                            {"fs": index},
+                        )
+                        pair_copies[j, h] = copy
+                        sent.append(copy)
+                for h in range(pieces):
+                    across(0, h)
+                strips(me)
+
+            def relay(h):
+                for j in range(1, n_pair):
+                    pair_copies[j, h].wait_recv()
+                    across(j, h)
+                    if h == pieces - 1:
+                        strips(rep * n_pair + lax.rem(p + n_pair - j, n_pair))
+
+            def complete(j):
+                for i in range(1, n_rep):
+                    for h in range(pieces):
+                        across_copies[i - 1, j, h].wait_recv()
+                    r = lax.rem(rep + n_rep - i, n_rep)
+                    strips(r * n_pair + lax.rem(p + n_pair - j, n_pair))
+
+            return begin, relay, complete, strip_copies
+
+        y_copies, x_copies, first_copies = {}, {}, []
+
+        def shard_of(e, d):
+            position = a if d == 0 else far[d - 1]
+            return position * inner + lax.rem(b + inner - e, inner)
+
+        def aside(k):
+            for e, index in enumerate(sides):
+                y_copies[k, e + 1] = send_to(
+                    origin(k, index),
+                    landing(k, fs),
+                    y_send.at[k, e],
+                    y_recv.at[k, e],
+                    {"fs": a * inner + index},
+                )
+                sent.append(y_copies[k, e + 1])
+            copy = pltpu.make_async_copy(
+                origin(k, b, 1), landing(k, fs, 1), first_sem.at[k]
+            )
+            copy.start()
+            first_copies.append(copy)
+
+        def along(k, e):
+            index = shard_of(e, 0)
+            start = landing(k, index) if e else origin(k, b)
+            if relayed:
+                middle = (jnp.where(between, 2, 1), jnp.where(between, far[2], far[1]))
+                steps = [(0, 0, far[0]), (1,) + middle]
+            else:
+                steps = [(d, d, far[d]) for d in every]
+            for d, slot, position in steps:
+                copy = send_to(
+                    start,
+                    landing(k, index),
+                    z_send.at[k, e, d],
+                    z_recv.at[k, e, slot],
+                    {"fs": position * inner + b},
+                )
+                sent.append(copy)
+
+        def line_copy(k, e, d, send_sem, slot):
+            landed = landing(k, shard_of(e, d + 1))
+            return pltpu.make_async_remote_copy(
+                src_ref=landed,
+                dst_ref=landed,
+                send_sem=send_sem,
+                recv_sem=z_recv.at[k, e, slot],
+                device_id={"fs": far[0] * inner + b},
+                device_id_type=MESH,
+            )
+
+        def passed_on(k, e, d):
+            return line_copy(k, e, d, pass_send.at[k, e, d], 3 - d)
+
+        def cross_plane(k, e, d):
+            landed = landing(k, shard_of(e, d))
+            for i, index in enumerate(reps):
+                x_copies[k, e, d, i] = send_to(
+                    landed,
+                    landed,
+                    x_send.at[k, e, d, i],
+                    x_recv.at[k, e, d, i],
+                    {"rep": index},
+                )
+                sent.append(x_copies[k, e, d, i])
+
+        def carry_on(k):
+            for d in every:
+                for e in range(inner):
+                    line_copy(k, e, d, z_send.at[k, e, d], d).wait_recv()
+                    if relayed and d > 0:
+                        passed.append((k, e, d))
+
+                        @pl.when(between)
+                        def _():
+                            passed_on(k, e, d).start()
+
+                    cross_plane(k, e, d + 1)
+
+        def settled(k):
+            first_copies[k].wait()
+            for (at_k, e, d, i), copy in x_copies.items():
+                if at_k == k:
+                    copy.wait_recv()
+
+        for k in range(len(firsts)):
+            aside(k)
+            along(k, 0)
+        spot = whole_ref.at[at(b * length, length), at(tp * columns, columns)]
         own_features = pltpu.make_async_copy(features_ref, spot, own_sem.at[count])
         own_features.start()
         group_copies = [
             send_to(features_ref, spot, group_send.at[d], group_recv.at[d], peer)
             for d, peer in enumerate(group)
         ]
-        lines = spike_all.at[at(rep * length, length), :]
+        lines = spike_all.at[at(b * length, length), :]
         own_spike = pltpu.make_async_copy(
-            spike_ref.at[:, at(rep * key_lanes, key_lanes)], lines, own_sem.at[count + 1]
+            spike_ref.at[:, at(b * key_lanes, key_lanes)], lines, own_sem.at[count + 1]
         )
         own_spike.start()
         group_copies += [
@@ -731,15 +919,29 @@
                 lines,
                 spike_send.at[d],
                 spike_recv.at[d],
-                {"rep": index},
+                {"fs": a * inner + index},
             )
-            for d, index in enumerate(reps)
+            for d, index in enumerate(sides)
         ]
-        for c in first:
-            launch_far(c)
+        for k in range(len(firsts)):
+            for e in range(1, inner):
+                y_copies[k, e].wait_recv()
+                along(k, e)
+                cross_plane(k, e, 0)
+        for c in third:
+            if relayed:
+                launch_middle(c)
+            else:
+                launch_far(c, every)
+        for c in third + fourth:
             launch_near(c)
-        for c in second + third:
-            launch_far(c)
+        for k in range(len(firsts)):
+            carry_on(k)
+        if relayed:
+            for c in third:
+                launch_end(c)
+            for c in fourth:
+                launch_middle(c)
         own_features.wait()
         own_spike.wait()
         for copy in group_copies:
@@ -750,38 +952,27 @@
             normed_ref[lines, :] = row_norm(whole_ref[lines, :], gain_ref[...])
             return carry
 
-        lax.fori_loop(0, n_rep, first_norm, 0)
-        for c in first:
-            forward(c)
-        half = len(third) // 2
-        for c in second + third[:half]:
-            launch_near(c)
-        for c in first:
-            arrived(c)
+        lax.fori_loop(0, inner, first_norm, 0)
+        for k in range(len(firsts)):
+            if firsts[k] != 5:
+                settled(k)
 
         def attention(index):
             lines = at(index * length, length)
             sums = jnp.dot(normed_ref[lines, :], project_all[...], preferred_element_type=F32)
             gated_ref[lines, :] = attend_rows(
                 sums,
-                shift_ref[:, at(rep * key_lanes, key_lanes)],
+                shift_ref[:, at(b * key_lanes, key_lanes)],
                 spike_all[lines, :],
-                scale_ref[:, at(rep * value_lanes, value_lanes)].astype(F32),
+                scale_ref[:, at(b * value_lanes, value_lanes)].astype(F32),
                 heads,
             )
 
-        order = reps + [rep]
-        attention(order[0])
-        for c in second:
-            forward(c)
-        for c in third[half:]:
-            launch_near(c)
-        for index in order[1:]:
+        half = len(third) // 2
+        order = sides + [b]
+        for index in order:
             attention(index)
-        for c in third[:half]:
-            forward(c)
-        for c in second:
-            arrived(c)
+        settled(firsts.index(5))
 
         def mixed(index, strip):
             return jnp.dot(
@@ -812,14 +1003,14 @@
             for d, copy in enumerate(mix_copies[i]):
                 copy.wait_recv()
                 total = total + slot_a[i, d].astype(F32)
-            if i < n_rep - 1:
+            if i < inner - 1:
                 held[i] = total.astype(BF16)
                 copy = send_to(
                     held.at[i],
                     slot_b.at[i],
                     cross_send.at[i],
                     cross_recv.at[i],
-                    {"rep": index},
+                    {"fs": a * inner + index},
                 )
                 cross_copies.append(copy)
                 sent.append(copy)
@@ -827,47 +1018,34 @@
                 for d, copy in enumerate(cross_copies):
                     copy.wait_recv()
                     total = total + slot_b[d].astype(F32)
-        base = whole_ref[at(rep * length, length), at(tp * columns, columns)].astype(F32)
+        base = whole_ref[at(b * length, length), at(tp * columns, columns)].astype(F32)
         mine = mid_all.at[at(me * length, length), at(tp * columns, columns)]
         mine[...] = (base + total.astype(BF16).astype(F32)).astype(BF16)
 
-        mid_copies = [
-            send_to(mine, mine, mid_send.at[k], mid_recv.at[k], peer)
-            for k, (peer, member) in enumerate(team)
-        ]
-        sent.extend(mid_copies)
-        strip_copies = []
-
-        def strips(k, member):
-            strip = mid_all.at[at(member * length, length), at(tp * columns, columns)]
-            copies = [
-                send_to(
-                    strip, strip, strip_send.at[k, d], strip_recv.at[k, d], {"tp": index}
-                )
-                for d, index in enumerate(tps)
-            ]
-            strip_copies.append(copies)
-            sent.extend(copies)
-
-        strips(0, me)
+        begin, relay, complete, blocks = spread(mid_all, second_spread)
+        begin()
         for c in fourth:
-            launch_far(c)
-        for c in third[half:]:
+            if relayed:
+                launch_end(c)
+            else:
+                launch_far(c, every)
+        for c in third:
             forward(c)
-        for c in fourth:
-            launch_near(c)
-        for k, member in enumerate(senders):
-            mid_copies[k].wait_recv()
-            strips(k + 1, member)
+        for h in range(pieces):
+            relay(h)
+        for j in range(n_pair):
+            complete(j)
 
         def second_norm(member):
             lines = at(member * length, length)
             normed_mid[lines, :] = row_norm(mid_all[lines, :], second_ref[...])
 
-        for k, member in enumerate([me] + senders):
-            for copy in strip_copies[k]:
+        for member, copies in blocks:
+            for copy in copies:
                 copy.wait_recv()
             second_norm(member)
+        for c in fourth:
+            forward(c)
         for c in third:
             arrived(c)
 
@@ -881,68 +1059,117 @@
             return carry
 
         lax.fori_loop(0, members, expand, 0)
-        for c in fourth:
-            forward(c)
-
-        back_copies = []
+
+        crossing = [
+            (i, j, index * n_pair + lax.rem(p + j, n_pair))
+            for j in reversed(range(n_pair))
+            for i, index in enumerate(reps)
+        ]
+        turn = len(crossing)
+
+        back_copies = {}
+        pending, turning = [], []
+
+        def finish(e, run, lanes, copies):
+            total = own_part[:, lanes]
+            for d, copy in enumerate(copies):
+                copy.wait_recv()
+                total = total + slot_d[d, :, lanes].astype(F32)
+            own_part[:, lanes] = total
+            held_down[:, lanes] = total.astype(BF16)
+            for k, (i, j, member) in enumerate(crossing):
+                back_copies[e, run, k] = send_to(
+                    held_down.at[at(member * length, length), lanes],
+                    slot_c.at[k, :, lanes],
+                    back_send.at[e, run, k],
+                    back_recv.at[e, run, k],
+                    {"rep": reps[i]},
+                )
+
+        def turned(e, run, lanes):
+            total = own_part[at(twin * length, length), lanes]
+            for k, (i, j, member) in enumerate(crossing):
+                if j:
+                    back_copies[e, run, k].wait_recv()
+                    total = total + slot_c[k, :, lanes].astype(F32)
+            held_twin[:, lanes] = total.astype(BF16)
+            back_copies[e, run, turn] = send_to(
+                held_twin.at[:, lanes],
+                slot_c.at[turn, :, lanes],
+                back_send.at[e, run, turn],
+                back_recv.at[e, run, turn],
+                twin_peer,
+            )
+
         for e in range(inner):
             lane = lax.rem(b + inner - e, inner)
-            for c in fourth:
-                if e == 0:
-                    own_copies[c].wait()
-                else:
-                    for d in range(outer):
-                        near_copies[c][d * (inner - 1) + e - 1].wait_recv()
-            spots = [at((run * inner + lane) * side, side) for run in range(runs)]
-
-            def product(strip, run):
-                index = (strip * runs + run) * inner + lane
+            waited = set()
+
+            def weights_of(run):
+                for c in fourth:
+                    for d in range(run, outer, runs) if aligned else range(outer):
+                        if (c, d) in waited:
+                            continue
+                        waited.add((c, d))
+                        if e:
+                            near_copies[c][d * (inner - 1) + e - 1].wait_recv()
+                        elif d == 0:
+                            own_copies[c].wait()
+
+            def spot(run):
+                place = lax.rem(p + run, runs) if aligned else run
+                return place, at((place * inner + lane) * side, side)
+
+            def product(strip, place):
+                index = (strip * runs + place) * inner + lane
                 return jnp.dot(
                     hidden_ref[...],
                     contract_all[:, at(index * side, side)],
                     preferred_element_type=F32,
                 )
 
-            down_copies = []
             for run in range(runs):
+                weights_of(run)
+                place, lanes = spot(run)
                 copies = []
                 for d, other in enumerate(tps):
-                    down_stage[d, :, spots[run]] = product(other, run).astype(BF16)
+                    down_stage[d, :, lanes] = product(other, place).astype(BF16)
                     copies.append(
                         send_to(
-                            down_stage.at[d, :, spots[run]],
-                            slot_d.at[d, :, spots[run]],
+                            down_stage.at[d, :, lanes],
+                            slot_d.at[d, :, lanes],
                             down_send.at[e, run, d],
                             down_recv.at[e, run, d],
                             {"tp": other},
                         )
                     )
-                down_copies.append(copies)
                 sent.extend(copies)
-            for run in range(runs):
-                total = product(tp, run)
-                for d, copy in enumerate(down_copies[run]):
-                    copy.wait_recv()
-                    total = total + slot_d[d, :, spots[run]].astype(F32)
-                own_part[:, spots[run]] = total
-                held_down[:, spots[run]] = total.astype(BF16)
-                for k, (peer, member) in enumerate(team):
-                    copy = send_to(
-                        held_down.at[at(member * length, length), spots[run]],
-                        slot_c.at[k, :, spots[run]],
-                        back_send.at[e, run, k],
-                        back_recv.at[e, run, k],
-                        peer,
-                    )
-                    back_copies.append(copy)
-        for copy in back_copies:
-            copy.wait_recv()
+                own_part[:, lanes] = product(tp, place)
+                for step in turning:
+                    turned(*step[:3])
+                turning = pending
+                for step in pending:
+                    finish(*step)
+                pending = [(e, run, lanes, copies)]
+        for step in pending:
+            finish(*step)
+        for step in turning + pending:
+            turned(*step[:3])
+        for (e, run, k), copy in back_copies.items():
+            if k == turn or not crossing[k][1]:
+                copy.wait_recv()
         total = own_part[at(me * length, length), :]
-        for k in range(members - 1):
+        for k in [turn] + [k for k in range(turn) if not crossing[k][1]]:
             total = total + slot_c[k].astype(F32)
         out_ref[...] = (mine[...].astype(F32) + total.astype(BF16).astype(F32)).astype(BF16)
-        for copy in sent + back_copies:
+        for copy in sent + list(back_copies.values()):
             copy.wait_send()
+        if passed:
+
+            @pl.when(between)
+            def _():
+                for step in passed:
+                    passed_on(*step).wait_send()
 
     dma = pltpu.SemaphoreType.DMA
     vmem = pl.BlockSpec(memory_space=pltpu.VMEM)
@@ -955,20 +1182,19 @@
     def room(*shape, dtype=BF16):
         return pltpu.VMEM(tuple(max(n, 1) for n in shape), dtype)
 
-    depth = weights[0].shape[0] * n_fs
     scratch = [
-        room(depth, sum(widths)),
-        room(part_rows[5], side * n_fs),
-        room(depth, 2 * units),
-        room(part_rows[8], side * n_fs),
+        room(shard * n_fs, sum(widths)),
+        room(result_rows, side * n_fs),
+        room(shard * n_fs, 2 * units),
+        room(down_rows, side * n_fs),
         room(rows, wide),
         room(rows, wide),
         room(rows, key_lanes, dtype=F32),
         room(rows, value_lanes),
-        room(n_rep, n_tp - 1, length, columns),
-        room(n_rep, n_tp - 1, length, columns),
-        room(n_rep - 1, length, columns),
-        room(n_rep - 1, length, columns),
+        room(inner, n_tp - 1, length, columns),
+        room(inner, n_tp - 1, length, columns),
+        room(inner - 1, length, columns),
+        room(inner - 1, length, columns),
         room(tokens, wide),
         room(tokens, wide),
         room(tokens, units),
@@ -979,10 +1205,14 @@
         room(members - 1, length, columns),
     ]
     scratch += pair(count, outer - 1) + pair(count, outer, inner - 1) + [dma((count + 2,))]
-    scratch += pair(n_rep * n_tp - 1) + pair(n_rep - 1)
-    scratch += pair(n_rep, n_tp - 1) + pair(n_rep - 1)
-    scratch += pair(members - 1) + pair(members, n_tp - 1)
+    many = len(firsts)
+    scratch += pair(inner - 1) + pair(inner, n_tp - 1) + pair(inner - 1)
+    scratch += pair(inner * n_tp - 1) + pair(many, inner - 1) + pair(many, inner, outer - 1)
+    scratch += pair(n_pair - 1, pieces) + pair(n_rep - 1, n_pair, pieces)
+    scratch += pair(members, n_tp - 1)
     scratch += pair(inner, runs, n_tp - 1) + pair(inner, runs, members - 1)
+    scratch += [dma((many, inner, max(outer - 1, 1))), room(length, columns)]
+    scratch += pair(many, inner, outer, n_rep - 1) + [dma((many,))]
     return pl.pallas_call(
         kernel,
         out_shape=jax.ShapeDtypeStruct((length, columns), BF16),

time: 179 us -> 152 us (0.85)
  Pallas kernels: 174 us -> 147 us
    pallas_call x1, Pallas kernels: 174 us -> 147 us  [whole_layer(): pl.pallas_call(kernel, out_shape=jax.ShapeDtypeStruct((length, columns),...]
where the time goes in v2:
time: 152 us; the launch traced here: 151 us
  Pallas kernels  147 us (97%)
  local copies, waits for them, and re-layouts  4.34 us (3%)
    pallas_call x1, Pallas kernels, whole_layer(): pl.pallas_call(kernel, out_shape=jax.ShapeDtypeStruct((length, columns),...  147 us

profile of v2, /device:TPU:0, one launch (start us, length us, event | category | flops | bytes accessed | tf_op | source)
XLA Modules:
  0.0 151.3 jit_solution(17933353629798448988)
XLA Ops:
  0.0 0.0 copy-start
  0.0 1.3 reshape.14.refs_13_
  1.3 0.0 copy-done
  1.3 0.0 copy-start.1
  1.3 0.6 reshape.12.refs_10_
  1.9 0.1 copy-done.1
  2.0 0.6 reshape.15.refs_14_
  2.6 147.0 %whole_layer.1 = bf16[192,1024]{1,0:T(8,128)(2,1)} custom-call(bf16[256,256]{1,0:T(8,128)(2,1)} %refs_0_.1, bf16[256,256]{1,0:T(8,128)(2,1)} %refs_1_.1, bf16[256,512]{1,0:T(8,128)(2,1)} %refs_2_.1, bf16[256,256]{1,0:T(8,128)(2,1)} %refs_3_.1, bf16[256,512]{1,0:T(8,128)(2,1)} %refs_4_.1, bf16[512,256]{1,0:T(8,128)(2,1)} %refs_5_.1, ...), custom_call_target="tpu_custom_call" | custom-call | tf_op jit(solution)/shard_map/whole_layer/pallas_call | solution.py:1216
  149.6 1.8 %copy.19 = bf16[192,1024]{1,0:T(8,128)(2,1)} copy(bf16[192,1024]{1,0:T(8,128)(2,1)} %whole_layer.1) | data formatting | bytes 786432
Async XLA Ops:
  0.0 1.3 copy-start
  1.3 0.7 copy-start.1

commit v3 on v2

--- a/solution.py
+++ b/solution.py
@@ -570,7 +570,7 @@
     side = weights[5].shape[1]
     runs = outer // n_tp
     aligned = runs == n_pair
-    pieces = pieces_of(length, 2)
+    pieces = pieces_of(length, 4)
 
     firsts = (0, 1, 3, 2, 4, 5)
     widths = [weights[w].shape[1] // inner for w in range(5)]
@@ -580,7 +580,7 @@
     down_rows = weights[8].shape[0] // members
     split = pieces_of(shard, 2)
     chunks = [(w, k * (shard // split), shard // split) for k in range(split) for w in (6, 7)]
-    split = pieces_of(down_rows, 2)
+    split = pieces_of(down_rows, members)
     size = down_rows // split
     chunks += [(8, k * size, size) for k in range(split)]
     count = len(chunks)
@@ -599,7 +599,7 @@
         (group_send, group_recv, y_send, y_recv, z_send, z_recv) = refs[49:55]
         second_spread = refs[55:61]
         (down_send, down_recv, back_send, back_recv, pass_send, held_twin) = refs[61:67]
-        (x_send, x_recv, first_sem) = refs[67:70]
+        (x_send, x_recv, first_sem, gain_rows) = refs[67:71]
         rep, fs, tp = lax.axis_index("rep"), lax.axis_index("fs"), lax.axis_index("tp")
         a, b = fs // inner, lax.rem(fs, inner)
         p = lax.rem(a, n_pair)
@@ -686,12 +686,35 @@
             for d in steps:
                 send_far(c, d, d, far[d])
 
-        def launch_middle(c):
+        def beside(c):
+            return pltpu.make_async_remote_copy(
+                src_ref=source(c, far[0]),
+                dst_ref=block(c, fs),
+                send_sem=far_send.at[c, 0],
+                recv_sem=far_recv.at[c, 0],
+                device_id={"fs": far[0] * inner + b},
+                device_id_type=MESH,
+            )
+
+        def launch_early(c):
+            if not relayed:
+                launch_far(c, every)
+                return
             send_far(c, 1, jnp.where(between, 2, 1), jnp.where(between, far[2], far[1]))
-
-        def launch_end(c):
+            sent.append(beside(c))
+
+            @pl.when(jnp.logical_not(between))
+            def _():
+                beside(c).start()
+
+        def launch_late(c):
+            if not relayed:
+                return
             send_far(c, 2, jnp.where(between, 1, 2), jnp.where(between, far[1], far[2]))
-            send_far(c, 0, 0, far[0])
+
+            @pl.when(between)
+            def _():
+                beside(c).start()
 
         def landed_far(c, d):
             landed = block(c, far[d] * inner + b)
@@ -716,25 +739,28 @@
                 )
                 for e, index in enumerate(near)
             ]
+            for d, position in enumerate(far):
+                landed = block(c, position * inner + b)
+                near_copies[c] += [
+                    pltpu.make_async_remote_copy(
+                        src_ref=landed,
+                        dst_ref=landed,
+                        send_sem=near_send.at[c, d + 1, e],
+                        recv_sem=near_recv.at[c, d + 1, e],
+                        device_id={"fs": index},
+                        device_id_type=MESH,
+                    )
+                    for e, index in enumerate(near)
+                ]
             sent.extend(near_copies[c])
             own_copies[c] = pltpu.make_async_copy(source(c, a), block(c, fs), own_sem.at[c])
             own_copies[c].start()
 
         def forward(c):
             for d in range(outer - 1):
-                landed = landed_far(c, d)
-                copies = [
-                    send_to(
-                        landed,
-                        landed,
-                        near_send.at[c, d + 1, e],
-                        near_recv.at[c, d + 1, e],
-                        {"fs": index},
-                    )
-                    for e, index in enumerate(near)
-                ]
-                near_copies[c] += copies
-                sent.extend(copies)
+                landed_far(c, d)
+                for e in range(inner - 1):
+                    near_copies[c][(d + 1) * (inner - 1) + e].start()
 
         def arrived(c):
             for copy in near_copies[c]:
@@ -822,8 +848,8 @@
         def aside(k):
             for e, index in enumerate(sides):
                 y_copies[k, e + 1] = send_to(
-                    origin(k, index),
-                    landing(k, fs),
+                    origin(k, index, 1),
+                    landing(k, fs, 1),
                     y_send.at[k, e],
                     y_recv.at[k, e],
                     {"fs": a * inner + index},
@@ -867,30 +893,37 @@
         def passed_on(k, e, d):
             return line_copy(k, e, d, pass_send.at[k, e, d], 3 - d)
 
-        def cross_plane(k, e, d):
-            landed = landing(k, shard_of(e, d))
-            for i, index in enumerate(reps):
-                x_copies[k, e, d, i] = send_to(
-                    landed,
-                    landed,
-                    x_send.at[k, e, d, i],
-                    x_recv.at[k, e, d, i],
-                    {"rep": index},
-                )
-                sent.append(x_copies[k, e, d, i])
-
-        def carry_on(k):
-            for d in every:
-                for e in range(inner):
-                    line_copy(k, e, d, z_send.at[k, e, d], d).wait_recv()
-                    if relayed and d > 0:
-                        passed.append((k, e, d))
-
-                        @pl.when(between)
-                        def _():
-                            passed_on(k, e, d).start()
-
-                    cross_plane(k, e, d + 1)
+        def carry_on(k, t, sources_of):
+            for e in sources_of:
+                slot, position = t, far[t]
+                if relayed:
+                    slot = jnp.where(between, 2 - t, t)
+                    position = jnp.where(between, far[2 - t], far[t])
+                landed = landing(k, position * inner + lax.rem(b + inner - e, inner))
+                pltpu.make_async_remote_copy(
+                    src_ref=landed,
+                    dst_ref=landed,
+                    send_sem=z_send.at[k, e, 0],
+                    recv_sem=z_recv.at[k, e, slot],
+                    device_id={"fs": far[0] * inner + b},
+                    device_id_type=MESH,
+                ).wait_recv()
+                if relayed and t < 2:
+                    passed.append((k, e, 2 - t))
+
+                    @pl.when(between)
+                    def _():
+                        passed_on(k, e, 2 - t).start()
+
+                for i, index in enumerate(reps):
+                    x_copies[k, e, t, i] = send_to(
+                        landed,
+                        landed,
+                        x_send.at[k, e, t, i],
+                        x_recv.at[k, e, t, i],
+                        {"rep": index},
+                    )
+                    sent.append(x_copies[k, e, t, i])
 
         def settled(k):
             first_copies[k].wait()
@@ -905,15 +938,21 @@
         own_features = pltpu.make_async_copy(features_ref, spot, own_sem.at[count])
         own_features.start()
         group_copies = [
-            send_to(features_ref, spot, group_send.at[d], group_recv.at[d], peer)
-            for d, peer in enumerate(group)
+            send_to(
+                features_ref,
+                spot,
+                group_send.at[e, 0],
+                group_recv.at[e, 0],
+                {"fs": a * inner + index},
+            )
+            for e, index in enumerate(sides)
         ]
         lines = spike_all.at[at(b * length, length), :]
         own_spike = pltpu.make_async_copy(
             spike_ref.at[:, at(b * key_lanes, key_lanes)], lines, own_sem.at[count + 1]
         )
         own_spike.start()
-        group_copies += [
+        spike_copies = [
             send_to(
                 spike_ref.at[:, at(index * key_lanes, key_lanes)],
                 lines,
@@ -927,32 +966,67 @@
             for e in range(1, inner):
                 y_copies[k, e].wait_recv()
                 along(k, e)
-                cross_plane(k, e, 0)
+            carry_on(k, 0, range(1))
         for c in third:
-            if relayed:
-                launch_middle(c)
-            else:
-                launch_far(c, every)
+            launch_early(c)
         for c in third + fourth:
             launch_near(c)
         for k in range(len(firsts)):
-            carry_on(k)
-        if relayed:
-            for c in third:
-                launch_end(c)
-            for c in fourth:
-                launch_middle(c)
+            carry_on(k, 0, range(1, inner))
         own_features.wait()
+        strip_copies = []
+        for e in range(inner):
+            if e:
+                group_copies[e - 1].wait()
+            strip = whole_ref.at[
+                at(lax.rem(b + inner - e, inner) * length, length), at(tp * columns, columns)
+            ]
+            strip_copies += [
+                send_to(
+                    strip, strip, group_send.at[e, d + 1], group_recv.at[e, d + 1], {"tp": index}
+                )
+                for d, index in enumerate(tps)
+            ]
+        for k in range(len(firsts)):
+            for t in every[1:]:
+                carry_on(k, t, range(inner))
+        gain_rows[...] = jnp.broadcast_to(
+            scale_ref[...].astype(F32).reshape(1, -1), gain_rows.shape
+        )
         own_spike.wait()
-        for copy in group_copies:
+        for copy in strip_copies + spike_copies:
             copy.wait()
 
         def first_norm(i, carry):
             lines = at(i * length, length)
-            normed_ref[lines, :] = row_norm(whole_ref[lines, :], gain_ref[...])
+            normed_ref[lines, :] = row_norm(whole_ref[lines, :], gain_ref[...].reshape(1, -1))
             return carry
 
         lax.fori_loop(0, inner, first_norm, 0)
+        for c in third:
+            launch_late(c)
+        for c in fourth:
+            launch_early(c)
+        def forwards(middle, ends):
+            if not relayed:
+                for c in ends:
+                    forward(c)
+                return
+
+            def each(chosen):
+                def send():
+                    for c in chosen:
+                        forward(c)
+
+                return send
+
+            if middle:
+                pl.when(between)(each(middle))
+            if ends:
+                pl.when(jnp.logical_not(between))(each(ends))
+
+        half = len(third) // 2
+        forwards(third[:half], [])
         for k in range(len(firsts)):
             if firsts[k] != 5:
                 settled(k)
@@ -964,13 +1038,12 @@
                 sums,
                 shift_ref[:, at(b * key_lanes, key_lanes)],
                 spike_all[lines, :],
-                scale_ref[:, at(b * value_lanes, value_lanes)].astype(F32),
+                gain_rows[:1, at(b * value_lanes, value_lanes)],
                 heads,
             )
 
-        half = len(third) // 2
         order = sides + [b]
-        for index in order:
+        for index in order[:1]:
             attention(index)
         settled(firsts.index(5))
 
@@ -981,11 +1054,12 @@
                 preferred_element_type=F32,
             )
 
-        mix_copies = []
-        for i, index in enumerate(order):
+        mix_copies, cross_copies = [], []
+
+        def mix_strips(i):
             copies = []
             for d, other in enumerate(tps):
-                stage[i, d] = mixed(index, other).astype(BF16)
+                stage[i, d] = mixed(order[i], other).astype(BF16)
                 copies.append(
                     send_to(
                         stage.at[i, d],
@@ -997,55 +1071,60 @@
                 )
             mix_copies.append(copies)
             sent.extend(copies)
-        cross_copies = []
-        for i, index in enumerate(order):
-            total = mixed(index, tp)
+
+        def mix_sum(i):
+            total = mixed(order[i], tp)
             for d, copy in enumerate(mix_copies[i]):
                 copy.wait_recv()
                 total = total + slot_a[i, d].astype(F32)
+            return total
+
+        for i in range(inner):
+            if i:
+                attention(order[i])
+            mix_strips(i)
             if i < inner - 1:
-                held[i] = total.astype(BF16)
+                held[i] = mix_sum(i).astype(BF16)
                 copy = send_to(
                     held.at[i],
                     slot_b.at[i],
                     cross_send.at[i],
                     cross_recv.at[i],
-                    {"fs": a * inner + index},
+                    {"fs": a * inner + order[i]},
                 )
                 cross_copies.append(copy)
                 sent.append(copy)
-            else:
-                for d, copy in enumerate(cross_copies):
-                    copy.wait_recv()
-                    total = total + slot_b[d].astype(F32)
+
+        forwards(third[half:], third[:1])
+        total = mix_sum(inner - 1)
+        for d, copy in enumerate(cross_copies):
+            copy.wait_recv()
+            total = total + slot_b[d].astype(F32)
         base = whole_ref[at(b * length, length), at(tp * columns, columns)].astype(F32)
         mine = mid_all.at[at(me * length, length), at(tp * columns, columns)]
         mine[...] = (base + total.astype(BF16).astype(F32)).astype(BF16)
 
         begin, relay, complete, blocks = spread(mid_all, second_spread)
         begin()
-        for c in fourth:
-            if relayed:
-                launch_end(c)
-            else:
-                launch_far(c, every)
-        for c in third:
-            forward(c)
+        forwards([], third[1:])
         for h in range(pieces):
             relay(h)
+        for c in fourth:
+            launch_late(c)
+        forwards(fourth, fourth[:1])
         for j in range(n_pair):
             complete(j)
 
         def second_norm(member):
             lines = at(member * length, length)
-            normed_mid[lines, :] = row_norm(mid_all[lines, :], second_ref[...])
-
+            normed_mid[lines, :] = row_norm(mid_all[lines, :], second_ref[...].reshape(1, -1))
+
+        forwards([], fourth[1:2])
         for member, copies in blocks:
             for copy in copies:
                 copy.wait_recv()
             second_norm(member)
-        for c in fourth:
-            forward(c)
+        forwards([], fourth[2:3])
         for c in third:
             arrived(c)
 
@@ -1058,48 +1137,54 @@
             hidden_ref[lines, :] = (value * jax.nn.gelu(gate, approximate=True)).astype(BF16)
             return carry
 
-        lax.fori_loop(0, members, expand, 0)
-
-        crossing = [
-            (i, j, index * n_pair + lax.rem(p + j, n_pair))
-            for j in reversed(range(n_pair))
-            for i, index in enumerate(reps)
-        ]
-        turn = len(crossing)
+        lax.fori_loop(0, 1, expand, 0)
+        forwards([], fourth[3:])
+        lax.fori_loop(1, members, expand, 0)
 
         back_copies = {}
         pending, turning = [], []
 
-        def finish(e, run, lanes, copies):
+        def finish(e, run, place, lanes, copies):
             total = own_part[:, lanes]
             for d, copy in enumerate(copies):
                 copy.wait_recv()
                 total = total + slot_d[d, :, lanes].astype(F32)
             own_part[:, lanes] = total
             held_down[:, lanes] = total.astype(BF16)
-            for k, (i, j, member) in enumerate(crossing):
+            for k, (i, j, member) in enumerate(phases(e, run)[0]):
                 back_copies[e, run, k] = send_to(
                     held_down.at[at(member * length, length), lanes],
                     slot_c.at[k, :, lanes],
-                    back_send.at[e, run, k],
-                    back_recv.at[e, run, k],
-                    {"rep": reps[i]},
+                    back_send.at[e, place, k],
+                    back_recv.at[e, place, k],
+                    peer_of(i, j),
                 )
 
-        def turned(e, run, lanes):
-            total = own_part[at(twin * length, length), lanes]
-            for k, (i, j, member) in enumerate(crossing):
-                if j:
+        def peer_of(i, j):
+            return {"rep": reps[i - 1]} if i else twin_peer
+
+        def phases(e, run):
+            def member(i, j):
+                return lax.rem(rep + i, n_rep) * n_pair + lax.rem(p + j, n_pair)
+
+            hops = [(i, 0, member(i, j)) for j in (1, 0) for i in range(1, n_rep)]
+            return hops, [(0, 1, member(0, 1))]
+
+        def turned(e, run, place, lanes):
+            hops, turns = phases(e, run)
+            for n, (i, j, member) in enumerate(turns):
+                total = own_part[at(member * length, length), lanes]
+                for k in range(n_rep - 1):
                     back_copies[e, run, k].wait_recv()
                     total = total + slot_c[k, :, lanes].astype(F32)
-            held_twin[:, lanes] = total.astype(BF16)
-            back_copies[e, run, turn] = send_to(
-                held_twin.at[:, lanes],
-                slot_c.at[turn, :, lanes],
-                back_send.at[e, run, turn],
-                back_recv.at[e, run, turn],
-                twin_peer,
-            )
+                held_twin[n, :, lanes] = total.astype(BF16)
+                back_copies[e, run, len(hops) + n] = send_to(
+                    held_twin.at[n, :, lanes],
+                    slot_c.at[len(hops) + n, :, lanes],
+                    back_send.at[e, place, len(hops) + n],
+                    back_recv.at[e, place, len(hops) + n],
+                    peer_of(i, j),
+                )
 
         for e in range(inner):
             lane = lax.rem(b + inner - e, inner)
@@ -1146,22 +1231,25 @@
                 sent.extend(copies)
                 own_part[:, lanes] = product(tp, place)
                 for step in turning:
-                    turned(*step[:3])
+                    turned(*step[:4])
                 turning = pending
                 for step in pending:
                     finish(*step)
-                pending = [(e, run, lanes, copies)]
+                pending = [(e, run, place, lanes, copies)]
         for step in pending:
             finish(*step)
         for step in turning + pending:
-            turned(*step[:3])
-        for (e, run, k), copy in back_copies.items():
-            if k == turn or not crossing[k][1]:
-                copy.wait_recv()
-        total = own_part[at(me * length, length), :]
-        for k in [turn] + [k for k in range(turn) if not crossing[k][1]]:
-            total = total + slot_c[k].astype(F32)
-        out_ref[...] = (mine[...].astype(F32) + total.astype(BF16).astype(F32)).astype(BF16)
+            turned(*step[:4])
+        for e in range(inner):
+            for run in range(runs):
+                lane = lax.rem(b + inner - e, inner)
+                lanes = at((lax.rem(p + run, runs) if aligned else run) * inner * side + lane * side, side)
+                total = own_part[at(me * length, length), lanes]
+                for k in range(n_rep - 1, members - 1):
+                    back_copies[e, run, k].wait_recv()
+                    total = total + slot_c[k, :, lanes].astype(F32)
+                base = mine[:, lanes].astype(F32)
+                out_ref[:, lanes] = (base + total.astype(BF16).astype(F32)).astype(BF16)
         for copy in sent + list(back_copies.values()):
             copy.wait_send()
         if passed:
@@ -1207,12 +1295,13 @@
     scratch += pair(count, outer - 1) + pair(count, outer, inner - 1) + [dma((count + 2,))]
     many = len(firsts)
     scratch += pair(inner - 1) + pair(inner, n_tp - 1) + pair(inner - 1)
-    scratch += pair(inner * n_tp - 1) + pair(many, inner - 1) + pair(many, inner, outer - 1)
+    scratch += pair(inner, n_tp) + pair(many, inner - 1) + pair(many, inner, outer - 1)
     scratch += pair(n_pair - 1, pieces) + pair(n_rep - 1, n_pair, pieces)
     scratch += pair(members, n_tp - 1)
     scratch += pair(inner, runs, n_tp - 1) + pair(inner, runs, members - 1)
-    scratch += [dma((many, inner, max(outer - 1, 1))), room(length, columns)]
-    scratch += pair(many, inner, outer, n_rep - 1) + [dma((many,))]
+    scratch += [dma((many, inner, max(outer - 1, 1))), room(n_rep - 1, length, columns)]
+    scratch += pair(many, inner, outer - 1, n_rep - 1) + [dma((many,))]
+    scratch.append(room(8, scale.shape[0], dtype=F32))
     return pl.pallas_call(
         kernel,
         out_shape=jax.ShapeDtypeStruct((length, columns), BF16),
@@ -1226,11 +1315,11 @@
     )(
         *weights,
         features,
-        first_gain.reshape(1, -1),
+        first_gain,
         shift.reshape(1, -1),
         spike,
-        scale.reshape(1, -1),
-        second_gain.reshape(1, -1),
+        scale,
+        second_gain,
         content_taps,
         switch_taps,
     )

time: 152 us -> 144 us (0.947)
  Pallas kernels: 147 us -> 142 us
  local copies, waits for them, and re-layouts: 4.34 us -> 1.77 us
    pallas_call x1, Pallas kernels: 147 us -> 142 us  [whole_layer(): pl.pallas_call(kernel, out_shape=jax.ShapeDtypeStruct((length, columns),...]
    reshape x3 -> x0, local copies, waits for them, and re-layouts: 2.48 us -> none  [the longest x1 1.27 us: whole_layer(): scale.reshape(1, -1)]
where the time goes in v3:
time: 144 us
  Pallas kernels  142 us (99%)
  local copies, waits for them, and re-layouts  1.77 us (1%)
    pallas_call x1, Pallas kernels, whole_layer(): pl.pallas_call(kernel, out_shape=jax.ShapeDtypeStruct((length, columns),...  142 us

profile of v3, /device:TPU:0, one launch (start us, length us, event | category | flops | bytes accessed | tf_op | source)
XLA Modules:
  0.0 144.1 jit_solution(17779722642603977434)
XLA Ops:
  0.0 142.3 %whole_layer.1 = bf16[192,1024]{1,0:T(8,128)(2,1)} custom-call(bf16[256,256]{1,0:T(8,128)(2,1)} %refs_0_.1, bf16[256,256]{1,0:T(8,128)(2,1)} %refs_1_.1, bf16[256,512]{1,0:T(8,128)(2,1)} %refs_2_.1, bf16[256,256]{1,0:T(8,128)(2,1)} %refs_3_.1, bf16[256,512]{1,0:T(8,128)(2,1)} %refs_4_.1, bf16[512,256]{1,0:T(8,128)(2,1)} %refs_5_.1, ...), custom_call_target="tpu_custom_call" | custom-call | tf_op jit(solution)/shard_map/whole_layer/pallas_call | solution.py:1305
  142.3 1.8 %copy.19 = bf16[192,1024]{1,0:T(8,128)(2,1)} copy(bf16[192,1024]{1,0:T(8,128)(2,1)} %whole_layer.1) | data formatting | bytes 786432
